TPU v7x, 256 devices: a whole 4x4x8 slice. The times are simulated.
256 devices in a mesh: sp: 64 (over z, x, core), tp: 4 (over y).
Axes of the slice: x: 4, y: 4, z: 8, core: 2. Of those that a mesh axis runs over, the one named last changes fastest.
Arguments:
- out_cotangent: bfloat16 [16384, 2048], P('sp'), may hold values from -16 to 16
- stream: bfloat16 [16384, 2048], P('sp'), may hold values from -6 to 6
- route_ids: int32 [16384, 2], P('sp'), may hold values from 0 to 63, all different within a row; in each aligned block of 256 rows (0 to 255, 256 to 511, ...) at most 16 rows name the same one
- route_weights: float32 [16384, 2], P('sp'), may hold values from 0.3 to 2
- gate_proj: bfloat16 [64, 2048, 1024], P('sp', None, 'tp'), may hold values from -0.125 to 0.125
- up_proj: bfloat16 [64, 2048, 1024], P('sp', None, 'tp'), may hold values from -0.125 to 0.125
- down_proj: bfloat16 [64, 1024, 2048], P('sp', 'tp'), may hold values from -0.1875 to 0.1875
- outer_gate: bfloat16 [16384, 512], P('sp', 'tp'), may hold values from -6 to 6
- inner_gate: bfloat16 [16384, 512], P('sp', 'tp'), may hold values from -6 to 6
- conv_input: bfloat16 [16384, 512], P('sp', 'tp'), may hold values from -6 to 6
- conv_taps: float32 [3, 512], P(None, 'tp'), may hold values from -4 to 4
- out_proj: bfloat16 [2048, 512], P(None, 'tp'), may hold values from -0.25 to 0.25
Outputs:
- grad_gate_proj: bfloat16 [64, 2048, 1024], P('sp', None, 'tp')
- grad_up_proj: bfloat16 [64, 2048, 1024], P('sp', None, 'tp')
- grad_down_proj: bfloat16 [64, 1024, 2048], P('sp', 'tp')
- grad_out_proj: float32 [2048, 512], P('sp', 'tp')
- grad_outer_gate: float32 [16384, 512], P('sp', 'tp')
- grad_inner_gate: float32 [16384, 512], P('sp', 'tp')
- grad_conv_input: float32 [16384, 512], P('sp', 'tp')
Inputs may be any that keep to these rules, and one draw needn't show every extreme that they name: `route_ids`: the 2 experts of a token differ. Among the tokens of one index of sp, no expert is chosen more than 16 times, and in every draw some expert is chosen exactly 16 times by them.
All inputs are finite; a program needn't handle non-finite values.
Results may differ from a plain program's by a relative error of at most 0.018.
Values may be sent and summed in bfloat16 or wider, within the bound.
No kernel may reach another device: no remote copies, remote signals or barrier semaphores. Data moves between devices by JAX's collectives and lax.ppermute only.
A program may use at most 64 MiB of HBM per device.

v0:
```python
import jax
import jax.numpy as jnp
from jax import lax
from jax.sharding import PartitionSpec as P


def sent_together(arrays, axis, dim, along):
    widths = [a.shape[along] for a in arrays]
    both = jnp.concatenate(arrays, axis=along)
    out = lax.all_gather(both, axis, axis=dim, tiled=True)
    return tuple(jnp.split(out, [sum(widths[:k]) for k in range(1, len(widths))], axis=along))


def in_blocks(x, dim, devices):
    before, after = (x.shape[:dim], x.shape[dim + 1 :])
    return jnp.moveaxis(x.reshape(*before, devices, -1, *after), dim, 0)


def summed_on_arrival(x, axis, dim):
    pieces = in_blocks(x, dim, lax.axis_size(axis))
    arrived = lax.all_to_all(pieces, axis, split_axis=0, concat_axis=0, tiled=True)
    return arrived.astype(jnp.float32).sum(axis=0)


def sent_to_all(x, axis):
    devices = lax.axis_size(axis)
    return lax.all_to_all(jnp.broadcast_to(x[None], (devices, *x.shape)), axis, 0, 0, tiled=True)


def in_order(pieces, dim):
    shape = list(pieces.shape[1:])
    shape[dim] *= pieces.shape[0]
    return jnp.moveaxis(pieces, 0, dim).reshape(shape)


def gathered_copies(x, axis, dim):
    pieces = sent_to_all(x, axis)
    return in_order(pieces, dim)


def passed_along(x, axis, by):
    devices = lax.axis_size(axis)
    pairs = [(i, i + by) for i in range(devices) if 0 <= i + by < devices]
    return lax.ppermute(x, axis, pairs)


def shards(
    out_cotangent,
    stream,
    route_ids,
    route_weights,
    gate_proj,
    up_proj,
    down_proj,
    outer_gate,
    inner_gate,
    conv_input,
    conv_taps,
    out_proj,
):
    sp_devices = lax.axis_size("sp")
    tokens_here, width = stream.shape
    choices_each = route_ids.shape[1]
    experts = sp_devices * gate_proj.shape[0]
    capacity = 4 * tokens_here // experts
    assigned = tokens_here * choices_each
    flat_expert = route_ids.reshape(-1)
    onehot = (flat_expert[:, None] == jnp.arange(experts, dtype=jnp.int32)[None, :]).astype(
        jnp.int32
    )
    earlier_count = jnp.cumsum(onehot, axis=0) - onehot
    slot_rank = jnp.sum(earlier_count * onehot, axis=1)
    destination = flat_expert * capacity + slot_rank
    slot_source = (
        jnp.full((experts * capacity,), assigned, jnp.int32)
        .at[destination]
        .set(jnp.arange(assigned, dtype=jnp.int32))
    )
    token_of = jnp.arange(assigned, dtype=jnp.int32) // choices_each
    scaled = (
        route_weights.reshape(-1)[:, None] * out_cotangent[token_of].astype(jnp.float32)
    ).astype(jnp.bfloat16)
    zero_row = jnp.zeros((1, width), jnp.bfloat16)
    send_grad = jnp.concatenate([scaled, zero_row], axis=0)[slot_source].reshape(
        sp_devices, capacity, width
    )
    slot_token = jnp.where(slot_source < assigned, slot_source // choices_each, tokens_here)
    send_input = jnp.concatenate([stream, zero_row], axis=0)[slot_token].reshape(
        sp_devices, capacity, width
    )
    columns = width // lax.axis_size("tp")
    offset = lax.axis_index("tp") * columns
    part_grad = lax.dynamic_slice_in_dim(send_grad, offset, columns, 2)
    part_input = lax.dynamic_slice_in_dim(send_input, offset, columns, 2)
    arrived_grad, arrived_input = (
        lax.all_to_all(part_grad, "sp", split_axis=0, concat_axis=0, tiled=True),
        lax.all_to_all(part_input, "sp", split_axis=0, concat_axis=0, tiled=True),
    )
    got_grad, got_input = sent_together((arrived_grad, arrived_input), "tp", 2, 0)
    rows_grad = got_grad.reshape(-1, width)
    rows_input = got_input.reshape(-1, width)
    w_gate = gate_proj[0]
    w_up = up_proj[0]
    w_down = down_proj[0]
    gate = jnp.dot(rows_input, w_gate, preferred_element_type=jnp.float32)
    up = jnp.dot(rows_input, w_up, preferred_element_type=jnp.float32)
    sig = jax.nn.sigmoid(gate)
    silu_gate = gate * sig
    hidden = (silu_gate * up).astype(jnp.bfloat16)
    across = (((1,), (1,)), ((), ()))
    d_hidden = lax.dot_general(rows_grad, w_down, across, preferred_element_type=jnp.float32)
    d_gate = (d_hidden * up * sig * (1.0 + gate * (1.0 - sig))).astype(jnp.bfloat16)
    d_up = (d_hidden * silu_gate).astype(jnp.bfloat16)
    over_rows = (((0,), (0,)), ((), ()))
    grad_down = lax.dot_general(
        hidden, rows_grad, over_rows, preferred_element_type=jnp.float32
    ).astype(jnp.bfloat16)
    grad_gate = lax.dot_general(
        rows_input, d_gate, over_rows, preferred_element_type=jnp.float32
    ).astype(jnp.bfloat16)
    grad_up = lax.dot_general(
        rows_input, d_up, over_rows, preferred_element_type=jnp.float32
    ).astype(jnp.bfloat16)
    partial_input = lax.dot_general(
        d_gate, w_gate, across, preferred_element_type=jnp.float32
    ) + lax.dot_general(d_up, w_up, across, preferred_element_type=jnp.float32)
    share = summed_on_arrival(partial_input.astype(jnp.bfloat16), "tp", 1).astype(jnp.bfloat16)
    quarter = share.shape[1]
    returned = lax.all_to_all(
        share.reshape(sp_devices, capacity, quarter), "sp", split_axis=0, concat_axis=0, tiled=True
    )
    per_assigned = returned.reshape(-1, quarter)[destination].astype(jnp.float32)
    moe_grad = jnp.sum(per_assigned.reshape(tokens_here, choices_each, quarter), axis=1)
    own_cotangent = lax.dynamic_slice_in_dim(
        out_cotangent, lax.axis_index("tp") * quarter, quarter, 1
    )
    stream_part = (own_cotangent.astype(jnp.float32) + moe_grad).astype(jnp.bfloat16)
    stream_grad = gathered_copies(stream_part, "tp", 1)
    mixed = inner_gate.astype(jnp.float32) * conv_input.astype(jnp.float32)
    previous = passed_along(mixed[tokens_here - 2 :], "sp", 1)
    extended = jnp.concatenate([previous, mixed], axis=0)
    conv_out = (
        conv_taps[0] * extended[:tokens_here]
        + conv_taps[1] * extended[1 : tokens_here + 1]
        + conv_taps[2] * extended[2:]
    )
    mixer_out = (outer_gate.astype(jnp.float32) * conv_out).astype(jnp.bfloat16)
    d_mixer = jnp.dot(stream_grad, out_proj, preferred_element_type=jnp.float32)
    grad_outer = d_mixer * conv_out
    d_conv = d_mixer * outer_gate.astype(jnp.float32)
    following = passed_along(d_conv[:2], "sp", -1)
    trailing = jnp.concatenate([d_conv, following], axis=0)
    d_mixed = (
        conv_taps[2] * trailing[:tokens_here]
        + conv_taps[1] * trailing[1 : tokens_here + 1]
        + conv_taps[0] * trailing[2:]
    )
    grad_inner = d_mixed * conv_input.astype(jnp.float32)
    grad_input = d_mixed * inner_gate.astype(jnp.float32)
    columns = stream_grad
    grad_projection = summed_on_arrival(
        lax.dot_general(columns, mixer_out, over_rows, preferred_element_type=jnp.float32).astype(
            jnp.bfloat16
        ),
        "sp",
        0,
    )
    return (
        grad_gate[None],
        grad_up[None],
        grad_down[None],
        grad_projection,
        grad_outer,
        grad_inner,
        grad_input,
    )


def solution(mesh):
    placed = (
        P("sp", None),
        P("sp", None),
        P("sp", None),
        P("sp", None),
        P("sp", None, "tp"),
        P("sp", None, "tp"),
        P("sp", "tp", None),
        P("sp", "tp"),
        P("sp", "tp"),
        P("sp", "tp"),
        P(None, "tp"),
        P(None, "tp"),
    )
    return jax.shard_map(
        shards,
        mesh=mesh,
        in_specs=placed,
        out_specs=(
            P("sp", None, "tp"),
            P("sp", None, "tp"),
            P("sp", "tp", None),
            P("sp", "tp"),
            P("sp", "tp"),
            P("sp", "tp"),
            P("sp", "tp"),
        ),
        check_vma=False,
    )
```

profile of v0, /device:TPU:1, one launch (start us, length us, event | category | flops | bytes accessed | tf_op | source)
XLA Modules:
  0.0 352.2 jit_solution(10132586161418526812)
XLA Ops:
  11.0 2.4 scatter_custom_fusion
  14.8 6.0 %gather_fusion.2 = bf16[1024,2048]{1,0:T(8,128)(2,1)} fusion(bf16[257,2048]{1,0:T(8,128)(2,1)S(1)} %concatenate.16, s32[1024]{0:T(1024)S(1)} %get-tuple-element.17), kind=kCustom, calls=%fused_computation.2 | custom fusion | bytes 8392704 | tf_op jit(solution)/shard_map/gather | solution.py:88
  20.8 2.4 constant_dynamic-slice_fusion
  23.2 13.2 %all-to-all-start.1 = ((bf16[64,16,512]{2,1,0:T(8,128)(2,1)}), bf16[64,16,512]{2,1,0:T(8,128)(2,1)}, u32[]{:S(2)}, u32[]{:S(2)}) async-start(bf16[64,16,512]{2,1,0:T(8,128)(2,1)} %constant_dynamic-slice_fusion), calls=%async_computation.1 | async-start | bytes 2097152 | tf_op jit(solution)/shard_map/all_to_all | solution.py:97
  36.7 3.3 gather_fusion
  42.3 6.0 %gather_fusion.1 = bf16[1024,2048]{1,0:T(8,128)(2,1)} fusion(bf16[513,2048]{1,0:T(8,128)(2,1)S(1)} %concatenate.15, s32[1024]{0:T(1024)S(1)} %get-tuple-element.16), kind=kCustom, calls=%fused_computation.1 | custom fusion | bytes 8392704 | tf_op jit(solution)/shard_map/gather | solution.py:84
  49.6 14.8 %all-to-all-done.1 = bf16[64,16,512]{2,1,0:T(8,128)(2,1)} async-done(((bf16[64,16,512]{2,1,0:T(8,128)(2,1)}), bf16[64,16,512]{2,1,0:T(8,128)(2,1)}, u32[]{:S(2)}, u32[]{:S(2)}) %all-to-all-start.1) | async-done | bytes 1048608 | tf_op jit(solution)/shard_map/all_to_all | solution.py:97
  64.4 34.2 %all_to_all.30 = bf16[64,16,512]{2,1,0:T(8,128)(2,1)S(1)} all-to-all(bf16[64,16,512]{2,1,0:T(8,128)(2,1)S(1)} %constant_dynamic-slice_fusion.1), channel_id=1, replica_groups=mesh['sp'=64,'tp'=4] {'sp'}, dimensions={0} | all-to-all | bytes 2097152 | tf_op jit(solution)/shard_map/all_to_all | solution.py:96
  98.6 2.8 pad_maximum_fusion
  101.4 82.7 %all-gather.2.cloned.1.call-done = bf16[128,16,2048]{2,1,0:T(8,128)(2,1)} async-done(((bf16[128,16,512]{2,1,0:T(8,128)(2,1)}), bf16[128,16,2048]{2,1,0:T(8,128)(2,1)}) %all-gather.2.cloned.1.call-update) | async-done | bytes 8388624 | tf_op jit(solution)/shard_map/all_gather | solution.py:10
  184.2 4.0 %fusion.41 = (bf16[64,16,2048]{2,1,0:T(8,128)(2,1)S(1)}, bf16[64,16,2048]{2,1,0:T(8,128)(2,1)S(1)}) fusion(bf16[128,16,2048]{2,1,0:T(8,128)(2,1)} %all-gather.2.cloned.1.call-done), kind=kLoop, calls=%fused_computation.93 | loop fusion | bytes 16777216 | tf_op jit(solution)/shard_map/split | solution.py:11
  196.8 51.4 %all_to_all.31 = bf16[4,1024,512]{2,1,0:T(8,128)(2,1)} all-to-all(bf16[4,1024,512]{2,1,0:T(8,128)(2,1)S(1)} %bitcast.81), channel_id=1, replica_groups=mesh['sp'=64,'tp'=4] {'tp'}, dimensions={0} | all-to-all | bytes 8388608 | tf_op jit(solution)/shard_map/all_to_all | solution.py:21
  248.2 4.1 %reduce_sum.43 = bf16[1024,512]{1,0:T(8,128)(2,1)} reduce(bf16[4,1024,512]{2,1,0:T(8,128)(2,1)} %all_to_all.31, bf16[]{:T(256)} %constant.49.clone.1), dimensions={0}, to_apply=%region_4.5 | reduce | flops 1572864 | bytes 5242882 | tf_op jit(solution)/shard_map/reduce_sum | solution.py:22
  252.3 12.0 %all-to-all-start.3 = ((bf16[64,16,512]{2,1,0:T(8,128)(2,1)}), bf16[64,16,512]{2,1,0:T(8,128)(2,1)S(1)}, u32[]{:S(2)}, u32[]{:S(2)}) async-start(bf16[64,16,512]{2,1,0:T(8,128)(2,1)} %bitcast.15), calls=%async_computation.3 | async-start | bytes 2097152 | tf_op jit(solution)/shard_map/all_to_all | solution.py:129
  264.3 28.1 %all-to-all-done.3 = bf16[64,16,512]{2,1,0:T(8,128)(2,1)S(1)} async-done(((bf16[64,16,512]{2,1,0:T(8,128)(2,1)}), bf16[64,16,512]{2,1,0:T(8,128)(2,1)S(1)}, u32[]{:S(2)}, u32[]{:S(2)}) %all-to-all-start.3) | async-done | bytes 1048608 | tf_op jit(solution)/shard_map/all_to_all | solution.py:129
  298.6 3.5 all-to-all-start.4
  302.2 4.1 %collective-permute-start = (f32[2,128]{1,0:T(2,128)S(1)}, f32[2,128]{1,0:T(2,128)S(1)}, u32[]{:S(2)}, u32[]{:S(2)}) collective-permute-start(f32[2,128]{1,0:T(2,128)S(1)} %slice.56), channel_id=1, source_target_pairs={{0,4},{4,8},{8,12},{12,16},{16,20},{20,24},{24,28},{28,32},{32,36}... | collective-permute-start | bytes 3080 | tf_op jit(solution)/shard_map/ppermute | solution.py:44
  306.4 5.1 %fusion.2 = bf16[1,256,2048]{2,1,0:T(8,128)(2,1)} fusion(bf16[1024,2048]{1,0:T(8,128)(2,1)} %bitcast.91, f32[1024,256]{1,0:T(8,128)} %copy-done.15, f32[1024,256]{1,0:T(8,128)} %copy-done.14), kind=kOutput, calls=%fused_computation.13 | convolution fusion | flops 1075838976 | bytes 7340032 | tf_op jit(solution)/shard_map/dot_general | solution.py:115
  311.5 4.6 %all-to-all-done.4 = bf16[4,256,512]{1,2,0:T(8,128)(2,1)S(1)} async-done(((bf16[4,256,512]{1,2,0:T(8,128)(2,1)}), bf16[4,256,512]{1,2,0:T(8,128)(2,1)S(1)}, u32[]{:S(2)}, u32[]{:S(2)}) %all-to-all-start.4) | async-done | bytes 1048608 | tf_op jit(solution)/shard_map/all_to_all | solution.py:27
  319.6 7.4 %all-to-all-start.5 = ((bf16[64,32,128]{2,1,0:T(8,128)(2,1)}), bf16[64,32,128]{2,1,0:T(8,128)(2,1)S(1)}, u32[]{:S(2)}, u32[]{:S(2)}) async-start(bf16[64,32,128]{2,1,0:T(8,128)(2,1)} %bitcast.22), calls=%async_computation.5 | async-start | bytes 1048576 | tf_op jit(solution)/shard_map/all_to_all | solution.py:21
  327.0 4.6 %fusion = bf16[1,2048,256]{2,1,0:T(8,128)(2,1)} fusion(bf16[1024,2048]{1,0:T(8,128)(2,1)} %bitcast.88, bf16[1024,256]{1,0:T(8,128)(2,1)S(1)} %get-tuple-element.14), kind=kOutput, calls=%fused_computation.11 | convolution fusion | flops 1074266112 | bytes 5767168 | tf_op jit(solution)/shard_map/dot_general | solution.py:118
  331.6 2.4 collective-permute-start.1
  334.0 2.4 fusion.1
  338.2 6.5 %all-to-all-done.5 = bf16[64,32,128]{2,1,0:T(8,128)(2,1)S(1)} async-done(((bf16[64,32,128]{2,1,0:T(8,128)(2,1)}), bf16[64,32,128]{2,1,0:T(8,128)(2,1)S(1)}, u32[]{:S(2)}, u32[]{:S(2)}) %all-to-all-start.5) | async-done | bytes 524320 | tf_op jit(solution)/shard_map/all_to_all | solution.py:21
  (81 shorter events, 29.6 us)
Async XLA Ops:
  7.2 181.0 %copy-start = (bf16[1,2048,256]{2,1,0:T(8,128)(2,1)S(1)}, bf16[1,2048,256]{2,1,0:T(8,128)(2,1)}, u32[]{:S(2)}) copy-start(bf16[1,2048,256]{2,1,0:T(8,128)(2,1)} %param.16) | copy-start | bytes 3145732
  20.8 15.6 %copy-start.11 = (f32[256,2]{0,1:T(2,128)S(1)}, f32[256,2]{0,1:T(2,128)}, u32[]{:S(2)}) copy-start(f32[256,2]{0,1:T(2,128)} %param.15) | copy-start | bytes 6148
  20.8 15.9 %copy-start.1 = (bf16[256,2048]{1,0:T(8,128)(2,1)S(1)}, bf16[256,2048]{1,0:T(8,128)(2,1)}, u32[]{:S(2)}) copy-start(bf16[256,2048]{1,0:T(8,128)(2,1)} %param.12) | copy-start | bytes 3145732
  23.2 41.3 %all-to-all-start.1 = ((bf16[64,16,512]{2,1,0:T(8,128)(2,1)}), bf16[64,16,512]{2,1,0:T(8,128)(2,1)}, u32[]{:S(2)}, u32[]{:S(2)}) async-start(bf16[64,16,512]{2,1,0:T(8,128)(2,1)} %constant_dynamic-slice_fusion), calls=%async_computation.1 | async-start | bytes 2097152 | tf_op jit(solution)/shard_map/all_to_all | solution.py:97
  36.3 147.8 %all-gather.2.cloned.1.call-start = ((), (), s32[]{:S(2)}) async-start(), calls=%async_computation.6 | async-start | bytes 10485760 | tf_op jit(solution)/shard_map/all_gather | solution.py:10
  188.2 3.3 copy-start.2
  188.2 3.4 copy-start.4
  188.2 2.0 copy-start.5
  190.2 3.5 %copy-start.14 = (f32[1024,256]{1,0:T(8,128)}, f32[1024,256]{1,0:T(8,128)S(1)}, u32[]{:S(2)}) copy-start(f32[1024,256]{1,0:T(8,128)S(1)} %fusion.5) | copy-start | bytes 3145732
  190.2 2.0 copy-start.13
  191.5 2.3 copy-start.15
  193.8 1.3 copy-start.6
  252.3 40.1 %all-to-all-start.3 = ((bf16[64,16,512]{2,1,0:T(8,128)(2,1)}), bf16[64,16,512]{2,1,0:T(8,128)(2,1)S(1)}, u32[]{:S(2)}, u32[]{:S(2)}) async-start(bf16[64,16,512]{2,1,0:T(8,128)(2,1)} %bitcast.15), calls=%async_computation.3 | async-start | bytes 2097152 | tf_op jit(solution)/shard_map/all_to_all | solution.py:129
  294.4 7.8 %copy-start.9 = (bf16[256,128]{1,0:T(8,128)(2,1)S(1)}, bf16[256,128]{1,0:T(8,128)(2,1)}, u32[]{:S(2)}) copy-start(bf16[256,128]{1,0:T(8,128)(2,1)} %param.21) | copy-start | bytes 196612
  294.4 7.8 %copy-start.10 = (bf16[256,128]{1,0:T(8,128)(2,1)S(1)}, bf16[256,128]{1,0:T(8,128)(2,1)}, u32[]{:S(2)}) copy-start(bf16[256,128]{1,0:T(8,128)(2,1)} %param.20) | copy-start | bytes 196612
  294.4 11.9 %copy-start.12 = (f32[3,128]{1,0:T(4,128)S(1)}, f32[3,128]{1,0:T(4,128)}, u32[]{:S(2)}) copy-start(f32[3,128]{1,0:T(4,128)} %param.22) | copy-start | bytes 4612
  298.6 17.5 %all-to-all-start.4 = ((bf16[4,256,512]{1,2,0:T(8,128)(2,1)}), bf16[4,256,512]{1,2,0:T(8,128)(2,1)S(1)}, u32[]{:S(2)}, u32[]{:S(2)}) async-start(bf16[4,256,512]{1,2,0:T(8,128)(2,1)} %broadcast_in_dim.36), calls=%async_computation.4 | async-start | bytes 2097152 | tf_op jit(solution)/shard_map/all_to_all | solution.py:27
  302.2 9.3 %collective-permute-start = (f32[2,128]{1,0:T(2,128)S(1)}, f32[2,128]{1,0:T(2,128)S(1)}, u32[]{:S(2)}, u32[]{:S(2)}) collective-permute-start(f32[2,128]{1,0:T(2,128)S(1)} %slice.56), channel_id=1, source_target_pairs={{0,4},{4,8},{8,12},{12,16},{16,20},{20,24},{24,28},{28,32},{32,36}... | collective-permute-start | bytes 3080 | tf_op jit(solution)/shard_map/ppermute | solution.py:44
  306.4 9.8 %copy-start.8 = (bf16[256,128]{1,0:T(8,128)(2,1)S(1)}, bf16[256,128]{1,0:T(8,128)(2,1)}, u32[]{:S(2)}) copy-start(bf16[256,128]{1,0:T(8,128)(2,1)} %param.19) | copy-start | bytes 196612
  319.6 25.1 %all-to-all-start.5 = ((bf16[64,32,128]{2,1,0:T(8,128)(2,1)}), bf16[64,32,128]{2,1,0:T(8,128)(2,1)S(1)}, u32[]{:S(2)}, u32[]{:S(2)}) async-start(bf16[64,32,128]{2,1,0:T(8,128)(2,1)} %bitcast.22), calls=%async_computation.5 | async-start | bytes 1048576 | tf_op jit(solution)/shard_map/all_to_all | solution.py:21
  327.0 7.0 %copy-start.3 = (bf16[64,16,2048]{2,1,0:T(8,128)(2,1)S(1)}, bf16[64,16,2048]{2,1,0:T(8,128)(2,1)}, u32[]{:S(2)}) copy-start(bf16[64,16,2048]{2,1,0:T(8,128)(2,1)} %copy-done.2) | copy-start | bytes 12582916
  327.0 7.0 %copy-start.7 = (bf16[1024,256]{1,0:T(8,128)(2,1)S(1)}, bf16[1024,256]{1,0:T(8,128)(2,1)}, u32[]{:S(2)}) copy-start(bf16[1024,256]{1,0:T(8,128)(2,1)} %copy-done.6) | copy-start | bytes 1572868
  331.6 5.2 %collective-permute-start.1 = (f32[2,128]{1,0:T(2,128)S(1)}, f32[2,128]{1,0:T(2,128)S(1)}, u32[]{:S(2)}, u32[]{:S(2)}) collective-permute-start(f32[2,128]{1,0:T(2,128)S(1)} %slice.59), channel_id=1, source_target_pairs={{4,0},{8,4},{12,8},{16,12},{20,16},{24,20},{28,24},{32,28},{36,32}... | collective-permute-start | bytes 3080 | tf_op jit(solution)/shard_map/ppermute | solution.py:44
Sparse Core Ops, SparseCore 0:
  101.6 82.5 all-gather.1
where the time goes:
time: 353 us; the launch traced here: 352 us
  waiting for transfers between devices  137 us (39%)
  blocking collectives  85.6 us (24%)
  starting transfers between devices  42.6 us (12%)
  local copies, waits for them, and re-layouts  34.6 us (10%)
  matrix products  22.2 us (6%)
  other arithmetic  15.4 us (4%)
  between operations  14.5 us (4%)
    all_gather x1, waiting for transfers between devices, sent_together(): out = lax.all_gather(both, axis, axis=dim, tiled=True)  82.7 us
    all_to_all x1, blocking collectives, summed_on_arrival(): lax.all_to_all(pieces, axis, split_axis=0, concat_axis=0, tiled=True)  51.4 us
    all_to_all x1, blocking collectives, shards(): lax.all_to_all(part_grad, 'sp', split_axis=0, concat_axis=0, tiled=True)  34.2 us
    all_to_all x1, waiting for transfers between devices, shards(): lax.all_to_all(share.reshape(sp_devices, capacity, quarter), 'sp', split_...  28.1 us
    all_to_all x1, waiting for transfers between devices, shards(): lax.all_to_all(part_input, 'sp', split_axis=0, concat_axis=0, tiled=True)  14.8 us
    all_to_all x1, starting transfers between devices, shards(): lax.all_to_all(part_input, 'sp', split_axis=0, concat_axis=0, tiled=True)  13.2 us
    all_to_all x1, starting transfers between devices, shards(): lax.all_to_all(share.reshape(sp_devices, capacity, quarter), 'sp', split_...  12 us
    all_to_all x1, starting transfers between devices, summed_on_arrival(): lax.all_to_all(pieces, axis, split_axis=0, concat_axis=0, tiled=True)  7.39 us
  transfers between devices with their start and end apart: 7, of which 6 were waited for; matrix products, arithmetic and copies ran while one was open for 8% of the time, Pallas kernels for 0%

commit v1 on v0

v1 whole, which is shorter than its diff:
```python
import functools

import jax
import jax.numpy as jnp
from jax import lax
from jax.experimental import pallas as pl
from jax.experimental.pallas import tpu as pltpu
from jax.sharding import PartitionSpec as P

F32 = jnp.float32
BF16 = jnp.bfloat16
OVER_ROWS = (((0,), (0,)), ((), ()))
ACROSS = (((1,), (1,)), ((), ()))


def dot(a, b, dims=(((1,), (0,)), ((), ()))):
    return lax.dot_general(a, b, dims, preferred_element_type=F32)


def whole(shape):
    return pl.BlockSpec(shape, lambda *_: (0,) * len(shape))


def cost(flops, bytes_accessed):
    return pl.CostEstimate(flops=flops, bytes_accessed=bytes_accessed, transcendentals=0)


def route_kernel(capacity, block, tp_ref, ids_ref, x_ref, dest_ref, out_ref):
    step = pl.program_id(0)
    tokens = ids_ref.shape[1]

    @pl.when(step == 0)
    def _():
        experts = out_ref.shape[0] * pl.num_programs(0) // capacity
        first, second = ids_ref[0:1, :], ids_ref[1:2, :]
        names = lax.broadcasted_iota(jnp.int32, (experts, tokens), 0)
        one = jnp.where(names == first, 1.0, 0.0)
        two = jnp.where(names == second, 1.0, 0.0)
        before = jnp.where(
            lax.broadcasted_iota(jnp.int32, (tokens, tokens), 0)
            < lax.broadcasted_iota(jnp.int32, (tokens, tokens), 1),
            1.0,
            0.0,
        ).astype(BF16)
        count_one = dot(one.astype(BF16), before)
        count_two = dot(two.astype(BF16), before) + jnp.sum(one, axis=1, keepdims=True)
        rank_one = jnp.sum(one * count_one, axis=0, keepdims=True).astype(jnp.int32)
        rank_two = jnp.sum(two * count_two, axis=0, keepdims=True).astype(jnp.int32)
        dest_ref[0:1, :] = first * capacity + rank_one
        dest_ref[1:2, :] = second * capacity + rank_two

    slots = lax.broadcasted_iota(jnp.int32, (block, tokens), 0) + step * block
    hit = (slots == dest_ref[0:1, :]) | (slots == dest_ref[1:2, :])
    out_ref[...] = dot(jnp.where(hit, 1.0, 0.0).astype(BF16), x_ref[...]).astype(BF16)


def scale_kernel(block, tp_ref, dest_ref, w_ref, x_ref, out_ref):
    tokens = dest_ref.shape[1]
    slots = lax.broadcasted_iota(jnp.int32, (block, tokens), 0) + pl.program_id(0) * block
    one = jnp.where(slots == dest_ref[0:1, :], 1.0, 0.0)
    two = jnp.where(slots == dest_ref[1:2, :], 1.0, 0.0)
    weight = jnp.sum(one * w_ref[0:1, :] + two * w_ref[1:2, :], axis=1, keepdims=True)
    rows = dot((one + two).astype(BF16), x_ref[...])
    out_ref[...] = (rows * weight).astype(BF16)


def quarter(tp, by, n):
    return lax.rem(tp + by, n)


def up_kernel(n, tp_ref, own, right, opp, left, wg_ref, wu_ref, gate_ref, up_ref, full_ref):
    tp = tp_ref[0]
    width = own.shape[1]
    gate = up = None
    for by, piece in enumerate((own, right, opp, left)):
        start = pl.multiple_of(quarter(tp, by, n) * width, width)
        x = piece[...]
        full_ref[:, pl.ds(start, width)] = x
        g = dot(x, wg_ref[pl.ds(start, width), :])
        u = dot(x, wu_ref[pl.ds(start, width), :])
        gate = g if gate is None else gate + g
        up = u if up is None else up + u
    gate_ref[...] = gate
    up_ref[...] = up


def down_kernel(
    n, tp_ref, own, right, opp, left, gate_ref, up_ref, wd_ref, wg_ref, wu_ref,
    hidden_ref, dgate_ref, dup_ref, own_out, right_out, opp_out, left_out, full_ref,
):
    tp = tp_ref[0]
    width = own.shape[1]
    d_hidden = None
    for by, piece in enumerate((own, right, opp, left)):
        start = pl.multiple_of(quarter(tp, by, n) * width, width)
        x = piece[...]
        full_ref[:, pl.ds(start, width)] = x
        d = dot(x, wd_ref[:, pl.ds(start, width)], ACROSS)
        d_hidden = d if d_hidden is None else d_hidden + d
    gate, up = gate_ref[...], up_ref[...]
    sig = jax.nn.sigmoid(gate)
    silu = gate * sig
    hidden_ref[...] = (silu * up).astype(BF16)
    d_gate = (d_hidden * up * sig * (1.0 + gate * (1.0 - sig))).astype(BF16)
    d_up = (d_hidden * silu).astype(BF16)
    dgate_ref[...] = d_gate
    dup_ref[...] = d_up
    for by, out in enumerate((own_out, right_out, opp_out, left_out)):
        start = pl.multiple_of(quarter(tp, by, n) * width, width)
        rows = dot(d_gate, wg_ref[pl.ds(start, width), :], ACROSS)
        rows = rows + dot(d_up, wu_ref[pl.ds(start, width), :], ACROSS)
        out[...] = rows.astype(BF16)


def sum_kernel(a0, a1, a2, b0, b1, b2, out_ref):
    out_ref[0] = (a0[...].astype(F32) + a1[...].astype(F32) + a2[...].astype(F32)).astype(BF16)
    out_ref[1] = (b0[...].astype(F32) + b1[...].astype(F32) + b2[...].astype(F32)).astype(BF16)


def token_kernel(
    n, tp_ref, dest_ref, back_ref, cot_ref, proj_ref, m_own, m_right, m_opp, m_left,
    mix_ref, grad_ref,
):
    tp = tp_ref[0]
    tokens = dest_ref.shape[1]
    slots = lax.broadcasted_iota(jnp.int32, (back_ref.shape[0], tokens), 0)
    hit = (slots == dest_ref[0:1, :]) | (slots == dest_ref[1:2, :])
    moe = dot(jnp.where(hit, 1.0, 0.0).astype(BF16), back_ref[...], OVER_ROWS)
    part = (cot_ref[...].astype(F32) + moe).astype(BF16)
    for block in range(n):
        mix_ref[block] = dot(part, proj_ref[block])
    for by, piece in enumerate((m_own, m_right, m_opp, m_left)):
        g = dot(part, piece[...], OVER_ROWS).astype(BF16)
        grad_ref[:, quarter(tp, by, n)] = g.reshape(grad_ref.shape[0], *grad_ref.shape[2:])


def shards(
    out_cotangent,
    stream,
    route_ids,
    route_weights,
    gate_proj,
    up_proj,
    down_proj,
    outer_gate,
    inner_gate,
    conv_input,
    conv_taps,
    out_proj,
):
    sp_devices = lax.axis_size("sp")
    n = lax.axis_size("tp")
    tp = lax.axis_index("tp").astype(jnp.int32)[None]
    tokens, width = stream.shape
    experts = sp_devices * gate_proj.shape[0]
    capacity = 4 * tokens // experts
    slots = experts * capacity
    q = width // n
    hidden_units = gate_proj.shape[2]
    channels = out_proj.shape[1]
    ahead = [(i, (i + 1) % n) for i in range(n)]
    back = [(i, (i - 1) % n) for i in range(n)]

    def to_right(x):
        return lax.ppermute(x, "tp", ahead)

    def to_left(x):
        return lax.ppermute(x, "tp", back)

    def over_sp(x):
        return lax.all_to_all(x, "sp", split_axis=0, concat_axis=0, tiled=True)

    ids = route_ids.T
    weights = route_weights.T
    block = 256
    steps = slots // block
    mine = pl.BlockSpec((tokens, q), lambda i, t: (0, t[0]))
    dest, send_x = pl.pallas_call(
        functools.partial(route_kernel, capacity, block),
        grid_spec=pltpu.PrefetchScalarGridSpec(
            num_scalar_prefetch=1,
            grid=(steps,),
            in_specs=[whole((2, tokens)), mine],
            out_specs=[whole((2, tokens)), pl.BlockSpec((block, q), lambda i, t: (i, 0))],
        ),
        out_shape=[
            jax.ShapeDtypeStruct((2, tokens), jnp.int32),
            jax.ShapeDtypeStruct((slots, q), BF16),
        ],
        cost_estimate=cost(2 * slots * tokens * q, 2 * (slots + tokens) * q),
        name="route",
    )(tp, ids, stream)
    got_x = over_sp(send_x.reshape(sp_devices, -1, q)).reshape(slots, q)
    send_c = pl.pallas_call(
        functools.partial(scale_kernel, block),
        grid_spec=pltpu.PrefetchScalarGridSpec(
            num_scalar_prefetch=1,
            grid=(steps,),
            in_specs=[whole((2, tokens)), whole((2, tokens)), mine],
            out_specs=pl.BlockSpec((block, q), lambda i, t: (i, 0)),
        ),
        out_shape=jax.ShapeDtypeStruct((slots, q), BF16),
        cost_estimate=cost(2 * slots * tokens * q, 2 * (slots + tokens) * q),
        name="scale",
    )(tp, dest, weights, out_cotangent)
    got_c = over_sp(send_c.reshape(sp_devices, -1, q)).reshape(slots, q)

    half = slots // 2

    def gathered(x):
        a, b = x[:half], x[half:]
        left_a, right_a = to_right(a), to_left(a)
        opp_a = to_right(left_a)
        right_b, left_b = to_left(b), to_right(b)
        opp_b = to_left(right_b)
        return (a, right_a, opp_a, left_a), (b, right_b, opp_b, left_b)

    w_gate, w_up, w_down = gate_proj[0], up_proj[0], down_proj[0]
    rows = 128
    piece = pl.BlockSpec((rows, q), lambda i, t: (i, 0))
    inner = pl.BlockSpec((rows, hidden_units), lambda i, t: (i, 0))
    wide = pl.BlockSpec((rows, width), lambda i, t: (i, 0))

    def expert_up(pieces):
        return pl.pallas_call(
            functools.partial(up_kernel, n),
            grid_spec=pltpu.PrefetchScalarGridSpec(
                num_scalar_prefetch=1,
                grid=(half // rows,),
                in_specs=[piece] * 4 + [whole(w_gate.shape)] * 2,
                out_specs=[inner, inner, wide],
            ),
            out_shape=[
                jax.ShapeDtypeStruct((half, hidden_units), F32),
                jax.ShapeDtypeStruct((half, hidden_units), F32),
                jax.ShapeDtypeStruct((half, width), BF16),
            ],
            cost_estimate=cost(4 * half * width * hidden_units, 4 * half * width),
            name="expert_up",
        )(tp, *pieces, w_gate, w_up)

    def expert_down(pieces, gate, up):
        return pl.pallas_call(
            functools.partial(down_kernel, n),
            grid_spec=pltpu.PrefetchScalarGridSpec(
                num_scalar_prefetch=1,
                grid=(half // rows,),
                in_specs=[piece] * 4
                + [inner] * 2
                + [whole(w_down.shape), whole(w_gate.shape), whole(w_up.shape)],
                out_specs=[inner] * 3 + [piece] * 4 + [wide],
            ),
            out_shape=[jax.ShapeDtypeStruct((half, hidden_units), BF16)] * 3
            + [jax.ShapeDtypeStruct((half, q), BF16)] * 4
            + [jax.ShapeDtypeStruct((half, width), BF16)],
            cost_estimate=cost(6 * half * width * hidden_units, 6 * half * width),
            name="expert_down",
        )(tp, *pieces, gate, up, w_down, w_gate, w_up)

    xa, xb = gathered(got_x)
    ca, cb = gathered(got_c)
    gate_a, up_a, x_a = expert_up(xa)
    gate_b, up_b, x_b = expert_up(xb)
    hid_a, dg_a, du_a, own_a, right_a, opp_a, left_a, c_a = expert_down(ca, gate_a, up_a)
    hid_b, dg_b, du_b, own_b, right_b, opp_b, left_b, c_b = expert_down(cb, gate_b, up_b)

    def added(x, y):
        return (x.astype(F32) + y.astype(F32)).astype(BF16)

    from_opp_a = to_right(opp_a)
    one_a = to_left(left_a)
    two_a = to_right(added(right_a, from_opp_a))
    from_opp_b = to_left(opp_b)
    one_b = to_right(right_b)
    two_b = to_left(added(left_b, from_opp_b))
    part = pl.BlockSpec((rows, q), lambda i: (i, 0))
    share = pl.pallas_call(
        sum_kernel,
        grid=(half // rows,),
        in_specs=[part] * 6,
        out_specs=pl.BlockSpec((2, rows, q), lambda i: (0, i, 0)),
        out_shape=jax.ShapeDtypeStruct((2, half, q), BF16),
        cost_estimate=cost(4 * slots * q, 8 * slots * q),
        name="share",
    )(own_a, one_a, two_a, own_b, one_b, two_b)
    returned = over_sp(share.reshape(sp_devices, -1, q)).reshape(slots, q)

    grad_gate = (dot(x_a, dg_a, OVER_ROWS) + dot(x_b, dg_b, OVER_ROWS)).astype(BF16)
    grad_up = (dot(x_a, du_a, OVER_ROWS) + dot(x_b, du_b, OVER_ROWS)).astype(BF16)
    grad_down = (dot(hid_a, c_a, OVER_ROWS) + dot(hid_b, c_b, OVER_ROWS)).astype(BF16)

    mixed = inner_gate.astype(F32) * conv_input.astype(F32)
    sp_ahead = [(i, i + 1) for i in range(sp_devices - 1)]
    sp_back = [(i + 1, i) for i in range(sp_devices - 1)]
    previous = lax.ppermute(mixed[tokens - 2 :], "sp", sp_ahead)
    extended = jnp.concatenate([previous, mixed], axis=0)
    conv_out = (
        conv_taps[0] * extended[:tokens]
        + conv_taps[1] * extended[1 : tokens + 1]
        + conv_taps[2] * extended[2:]
    )
    mixer_out = (outer_gate.astype(F32) * conv_out).astype(BF16)
    mixer_left = to_right(mixer_out)
    mixer_right = to_left(mixer_out)
    mixer_opp = to_right(mixer_left)
    proj_rows = lax.all_to_all(out_proj.reshape(n, q, channels), "tp", 0, 0, tiled=True)

    strip = width // sp_devices
    row_blocks = q // strip
    partial_mix, partial_grad = pl.pallas_call(
        functools.partial(token_kernel, n),
        grid_spec=pltpu.PrefetchScalarGridSpec(
            num_scalar_prefetch=1,
            grid=(1,),
            in_specs=[
                whole((2, tokens)),
                whole((slots, q)),
                mine,
                whole((n, q, channels)),
            ]
            + [whole((tokens, channels))] * 4,
            out_specs=[whole((n, tokens, channels)), whole((row_blocks, n, strip, channels))],
        ),
        out_shape=[
            jax.ShapeDtypeStruct((n, tokens, channels), F32),
            jax.ShapeDtypeStruct((row_blocks, n, strip, channels), BF16),
        ],
        cost_estimate=cost(2 * slots * tokens * q + 16 * tokens * q * channels, 4 * slots * q),
        name="token",
    )(
        tp, dest, returned, out_cotangent, proj_rows,
        mixer_out, mixer_right, mixer_opp, mixer_left,
    )
    summed = over_sp(partial_grad.reshape(sp_devices, strip, channels)).astype(F32).sum(axis=0)
    home = [
        (s * n + t, (row_blocks * t + s // n) * n + s % n)
        for s in range(sp_devices)
        for t in range(n)
    ]
    grad_projection = lax.ppermute(summed, ("sp", "tp"), home)

    d_mixer = lax.all_to_all(partial_mix, "tp", 0, 0, tiled=True).sum(axis=0)
    grad_outer = d_mixer * conv_out
    d_conv = d_mixer * outer_gate.astype(F32)
    following = lax.ppermute(d_conv[:2], "sp", sp_back)
    trailing = jnp.concatenate([d_conv, following], axis=0)
    d_mixed = (
        conv_taps[2] * trailing[:tokens]
        + conv_taps[1] * trailing[1 : tokens + 1]
        + conv_taps[0] * trailing[2:]
    )
    grad_inner = d_mixed * conv_input.astype(F32)
    grad_input = d_mixed * inner_gate.astype(F32)
    return (
        grad_gate[None],
        grad_up[None],
        grad_down[None],
        grad_projection,
        grad_outer,
        grad_inner,
        grad_input,
    )


def solution(mesh):
    placed = (
        P("sp", None),
        P("sp", None),
        P("sp", None),
        P("sp", None),
        P("sp", None, "tp"),
        P("sp", None, "tp"),
        P("sp", "tp", None),
        P("sp", "tp"),
        P("sp", "tp"),
        P("sp", "tp"),
        P(None, "tp"),
        P(None, "tp"),
    )
    return jax.shard_map(
        shards,
        mesh=mesh,
        in_specs=placed,
        out_specs=(
            P("sp", None, "tp"),
            P("sp", None, "tp"),
            P("sp", "tp", None),
            P("sp", "tp"),
            P("sp", "tp"),
            P("sp", "tp"),
            P("sp", "tp"),
        ),
        check_vma=False,
    )
```

time: 353 us -> 293 us (0.83)
  blocking collectives: 85.6 us -> 0 us
  starting transfers between devices: 42.6 us -> 93.4 us
  Pallas kernels: 0 us -> 45.2 us
  local copies, waits for them, and re-layouts: 34.6 us -> 6.54 us
  between operations: 14.5 us -> 1.08 us
  matrix products: 22.2 us -> 10.7 us
  other arithmetic: 15.4 us -> 5.25 us
  waiting for transfers between devices: 137 us -> 127 us
    all_to_all x2 -> x0, blocking collectives: 85.6 us -> none  [the longest x1 51.4 us: summed_on_arrival(): lax.all_to_all(pieces, axis, split_axis=0, concat_axis=0, tiled=True)]
    all_gather x1 -> x0, waiting for transfers between devices: 82.7 us -> none  [sent_together(): out = lax.all_gather(both, axis, axis=dim, tiled=True)]
    ppermute x2 -> x24, waiting for transfers between devices: 0.43 us -> 53 us  [the longest x10 34.3 us: to_left(): return lax.ppermute(x, 'tp', back)]
    pallas_call x0 -> x8, Pallas kernels: none -> 45.2 us  [the longest x2 19.9 us: expert_down(): pl.pallas_call(functools.partial(down_kernel, n), grid_spec=pltpu.Prefetc...]
    ppermute x2 -> x24, starting transfers between devices: 6.49 us -> 35.3 us  [the longest x10 18.9 us: to_left(): return lax.ppermute(x, 'tp', back)]
    all_to_all x4 -> x6, starting transfers between devices: 36 us -> 58.1 us  [the longest x4 49.9 us: over_sp(): return lax.all_to_all(x, 'sp', split_axis=0, concat_axis=0, tiled=True)]
    all_to_all x4 -> x6, waiting for transfers between devices: 54.1 us -> 74 us  [the longest x4 69.5 us: over_sp(): return lax.all_to_all(x, 'sp', split_axis=0, concat_axis=0, tiled=True)]
    gather x4 -> x0, local copies, waits for them, and re-layouts: 17.3 us -> none  [the longest x1 6.01 us: shards(): jnp.concatenate([stream, zero_row], axis=0)[slot_token]]
  transfers between devices with their start and end apart: 7 -> 30, of which waited for: 6 -> 16; matrix products, arithmetic and copies ran while one was open for 8% -> 6% of each run, Pallas kernels for 0% -> 13%
where the time goes in v1:
time: 293 us; the launch traced here: 289 us
  waiting for transfers between devices  127 us (43%)
  starting transfers between devices  93.4 us (32%)
  Pallas kernels  45.2 us (15%)
  matrix products  10.7 us (4%)
  local copies, waits for them, and re-layouts  6.54 us (2%)
  other arithmetic  5.25 us (2%)
    all_to_all x4, waiting for transfers between devices, over_sp(): return lax.all_to_all(x, 'sp', split_axis=0, concat_axis=0, tiled=True)  69.5 us
    all_to_all x4, starting transfers between devices, over_sp(): return lax.all_to_all(x, 'sp', split_axis=0, concat_axis=0, tiled=True)  49.9 us
    ppermute x10, waiting for transfers between devices, to_left(): return lax.ppermute(x, 'tp', back)  34.3 us
    pallas_call x2, Pallas kernels, expert_down(): pl.pallas_call(functools.partial(down_kernel, n), grid_spec=pltpu.Prefetc...  19.9 us
    ppermute x10, starting transfers between devices, to_left(): return lax.ppermute(x, 'tp', back)  18.9 us
    ppermute x11, waiting for transfers between devices, to_right(): return lax.ppermute(x, 'tp', ahead)  14.5 us
    pallas_call x2, Pallas kernels, expert_up(): pl.pallas_call(functools.partial(up_kernel, n), grid_spec=pltpu.PrefetchS...  11.4 us
    dot_general x6, matrix products, dot(): return lax.dot_general(a, b, dims, preferred_element_type=F32)  10.7 us
  transfers between devices with their start and end apart: 30, of which 16 were waited for; matrix products, arithmetic and copies ran while one was open for 6% of the time, Pallas kernels for 13%

profile of v1, /device:TPU:1, one launch (start us, length us, event | category | flops | bytes accessed | tf_op | source)
XLA Modules:
  0.0 289.2 jit_solution(1547464304942603772)
XLA Ops:
  4.0 13.0 %all-to-all-start = ((bf16[64,16,512]{2,1,0:T(8,128)(2,1)}), bf16[64,16,512]{2,1,0:T(8,128)(2,1)S(1)}, u32[]{:S(2)}, u32[]{:S(2)}) async-start(bf16[64,16,512]{2,1,0:T(8,128)(2,1)} %bitcast.65), calls=%async_computation | async-start | bytes 2097152 | tf_op jit(solution)/shard_map/all_to_all | solution.py:171
  20.1 25.0 %all-to-all-done = bf16[64,16,512]{2,1,0:T(8,128)(2,1)S(1)} async-done(((bf16[64,16,512]{2,1,0:T(8,128)(2,1)}), bf16[64,16,512]{2,1,0:T(8,128)(2,1)S(1)}, u32[]{:S(2)}, u32[]{:S(2)}) %all-to-all-start) | async-done | bytes 1048608 | tf_op jit(solution)/shard_map/all_to_all | solution.py:171
  45.1 6.3 %all-to-all-start.1 = ((bf16[64,16,512]{2,1,0:T(8,128)(2,1)}), bf16[64,16,512]{2,1,0:T(8,128)(2,1)S(1)}, u32[]{:S(2)}, u32[]{:S(2)}) async-start(bf16[64,16,512]{2,1,0:T(8,128)(2,1)} %bitcast.50), calls=%async_computation.1 | async-start | bytes 2097152 | tf_op jit(solution)/shard_map/all_to_all | solution.py:171
  54.4 25.2 %all-to-all-done.1 = bf16[64,16,512]{2,1,0:T(8,128)(2,1)S(1)} async-done(((bf16[64,16,512]{2,1,0:T(8,128)(2,1)}), bf16[64,16,512]{2,1,0:T(8,128)(2,1)S(1)}, u32[]{:S(2)}, u32[]{:S(2)}) %all-to-all-start.1) | async-done | bytes 1048608 | tf_op jit(solution)/shard_map/all_to_all | solution.py:171
  85.4 8.1 %collective-permute-done.4.left = bf16[512,512]{1,0:T(8,128)(2,1)} collective-permute-done((bf16[512,512]{1,0:T(8,128)(2,1)S(1)}, bf16[512,512]{1,0:T(8,128)(2,1)}, u32[]{:S(2)}, u32[]{:S(2)}) %collective-permute-start.4) | collective-permute-done | bytes 524320 | tf_op jit(solution)/shard_map/ppermute | solution.py:165
  94.8 9.5 %collective-permute-done.6.right = bf16[512,512]{1,0:T(8,128)(2,1)S(1)} collective-permute-done((bf16[512,512]{1,0:T(8,128)(2,1)S(1)}, bf16[512,512]{1,0:T(8,128)(2,1)S(1)}, u32[]{:S(2)}, u32[]{:S(2)}) %collective-permute-start.6) | collective-permute-done | bytes 524320 | tf_op jit(solution)/shard_map/ppermute | solution.py:168
  107.2 8.4 %collective-permute-done.9.right = bf16[512,512]{1,0:T(8,128)(2,1)S(1)} collective-permute-done((bf16[512,512]{1,0:T(8,128)(2,1)S(1)}, bf16[512,512]{1,0:T(8,128)(2,1)S(1)}, u32[]{:S(2)}, u32[]{:S(2)}) %collective-permute-start.9) | collective-permute-done | bytes 524320 | tf_op jit(solution)/shard_map/ppermute | solution.py:168
  119.3 5.7 %expert_up.2 = (f32[512,256]{1,0:T(8,128)}, f32[512,256]{1,0:T(8,128)}, bf16[512,2048]{1,0:T(8,128)(2,1)}) custom-call(s32[1]{0:T(128)} %bitcast.tp_ref, bf16[512,512]{1,0:T(8,128)(2,1)} %bitcast.61, bf16[512,512]{1,0:T(8,128)(2,1)} %collective-permute-done.right, bf16[512,512]{1,0:T(8,128)(2,1)} %copy-done.13, ...), custom_call_target="tpu_custom_call" | custom-call | flops 1073741824 | bytes 4194304 | tf_op jit(solution)/shard_map/expert_up/pallas_call | solution.py:225
  125.0 10.0 %expert_down.2 = (bf16[512,256]{1,0:T(8,128)(2,1)}, bf16[512,256]{1,0:T(8,128)(2,1)}, bf16[512,256]{1,0:T(8,128)(2,1)}, bf16[512,512]{1,0:T(8,128)(2,1)}, bf16[5...) custom-call(s32[1]{0:T(128)} %bitcast.tp_ref, ...), custom_call_target="tpu_custom_call" | custom-call | flops 1610612736 | bytes 6291456 | tf_op jit(solution)/shard_map/expert_down/pallas_call | solution.py:243
  135.1 5.7 %expert_up.3 = (f32[512,256]{1,0:T(8,128)}, f32[512,256]{1,0:T(8,128)}, bf16[512,2048]{1,0:T(8,128)(2,1)}) custom-call(s32[1]{0:T(128)} %bitcast.tp_ref, bf16[512,512]{1,0:T(8,128)(2,1)} %bitcast.58, bf16[512,512]{1,0:T(8,128)(2,1)} %copy-done.10, bf16[512,512]{1,0:T(8,128)(2,1)} %collective-permute-done.7.opp, ...), custom_call_target="tpu_custom_call" | custom-call | flops 1073741824 | bytes 4194304 | tf_op jit(solution)/shard_map/expert_up/pallas_call | solution.py:225
  140.9 9.9 %expert_down.3 = (bf16[512,256]{1,0:T(8,128)(2,1)}, bf16[512,256]{1,0:T(8,128)(2,1)}, bf16[512,256]{1,0:T(8,128)(2,1)}, bf16[512,512]{1,0:T(8,128)(2,1)}, bf16[5...) custom-call(s32[1]{0:T(128)} %bitcast.tp_ref, ...), custom_call_target="tpu_custom_call" | custom-call | flops 1610612736 | bytes 6291456 | tf_op jit(solution)/shard_map/expert_down/pallas_call | solution.py:243
  155.2 5.1 %collective-permute-done.16 = bf16[512,512]{1,0:T(8,128)(2,1)S(1)} collective-permute-done((bf16[512,512]{1,0:T(8,128)(2,1)}, bf16[512,512]{1,0:T(8,128)(2,1)S(1)}, u32[]{:S(2)}, u32[]{:S(2)}) %collective-permute-start.16) | collective-permute-done | bytes 524320 | tf_op jit(solution)/shard_map/ppermute | solution.py:168
  164.9 3.5 %all-to-all-start.3 = ((bf16[4,512,128]{2,1,0:T(8,128)(2,1)}), bf16[4,512,128]{2,1,0:T(8,128)(2,1)S(1)}, u32[]{:S(2)}, u32[]{:S(2)}) async-start(bf16[4,512,128]{2,1,0:T(8,128)(2,1)} %bitcast.17), calls=%async_computation.3 | async-start | bytes 1048576 | tf_op jit(solution)/shard_map/all_to_all | solution.py:306
  174.7 8.0 %collective-permute-done.17.b2 = bf16[512,512]{1,0:T(8,128)(2,1)S(1)} collective-permute-done((bf16[512,512]{1,0:T(8,128)(2,1)S(1)}, bf16[512,512]{1,0:T(8,128)(2,1)S(1)}, u32[]{:S(2)}, u32[]{:S(2)}) %collective-permute-start.17) | collective-permute-done | bytes 524320 | tf_op jit(solution)/shard_map/ppermute | solution.py:168
  183.6 4.0 %share.1 = bf16[2,512,512]{2,1,0:T(8,128)(2,1)} custom-call(bf16[512,512]{1,0:T(8,128)(2,1)} %get-tuple-element.49.a0, bf16[512,512]{1,0:T(8,128)(2,1)} %copy-done.14, bf16[512,512]{1,0:T(8,128)(2,1)} %copy-done.15, bf16[512,512]{1,0:T(8,128)(2,1)} %get-tuple-element.53.b0, bf16[512,512]{1,0:T(8,128)(2,1)} %collective-permute-done.15.b1, ...), custom_call_target="tpu_custom_call" | custom-call | flops 2097152 | bytes 4194304 | tf_op jit(solution)/shard_map/share/pallas_call | solution.py:277
  188.4 14.7 %all-to-all-start.2 = ((bf16[64,16,512]{2,1,0:T(8,128)(2,1)}), bf16[64,16,512]{2,1,0:T(8,128)(2,1)S(1)}, u32[]{:S(2)}, u32[]{:S(2)}) async-start(bf16[64,16,512]{2,1,0:T(8,128)(2,1)} %bitcast.51), calls=%async_computation.2 | async-start | bytes 2097152 | tf_op jit(solution)/shard_map/all_to_all | solution.py:171
  203.2 3.5 %collective-permute-start.18 = (f32[2,128]{1,0:T(2,128)S(1)}, f32[2,128]{1,0:T(2,128)S(1)}, u32[]{:S(2)}, u32[]{:S(2)}) collective-permute-start(f32[2,128]{1,0:T(2,128)S(1)} %slice.75), channel_id=1, source_target_pairs={{0,4},{4,8},{8,12},{12,16},{16,20},{20,24},{24,28},{28,32},{32,36}... | collective-permute-start | bytes 3080 | tf_op jit(solution)/shard_map/ppermute | solution.py:295
  219.2 12.1 %all-to-all-done.2 = bf16[64,16,512]{2,1,0:T(8,128)(2,1)S(1)} async-done(((bf16[64,16,512]{2,1,0:T(8,128)(2,1)}), bf16[64,16,512]{2,1,0:T(8,128)(2,1)S(1)}, u32[]{:S(2)}, u32[]{:S(2)}) %all-to-all-start.2) | async-done | bytes 1048608 | tf_op jit(solution)/shard_map/all_to_all | solution.py:171
  235.6 4.7 %all-to-all-start.5 = ((f32[4,256,128]{2,1,0:T(8,128)}), f32[4,256,128]{2,1,0:T(8,128)S(1)}, u32[]{:S(2)}, u32[]{:S(2)}) async-start(f32[4,256,128]{2,1,0:T(8,128)} %get-tuple-element.58), calls=%async_computation.5 | async-start | bytes 1048576 | tf_op jit(solution)/shard_map/all_to_all | solution.py:342
  243.6 4.5 %all-to-all-done.5 = f32[4,256,128]{2,1,0:T(8,128)S(1)} async-done(((f32[4,256,128]{2,1,0:T(8,128)}), f32[4,256,128]{2,1,0:T(8,128)S(1)}, u32[]{:S(2)}, u32[]{:S(2)}) %all-to-all-start.5) | async-done | bytes 524320 | tf_op jit(solution)/shard_map/all_to_all | solution.py:342
  248.1 16.0 %all-to-all-start.4 = ((bf16[64,32,128]{2,1,0:T(8,128)(2,1)}), bf16[64,32,128]{2,1,0:T(8,128)(2,1)S(1)}, u32[]{:S(2)}, u32[]{:S(2)}) async-start(bf16[64,32,128]{2,1,0:T(8,128)(2,1)} %bitcast.21), calls=%async_computation.4 | async-start | bytes 1048576 | tf_op jit(solution)/shard_map/all_to_all | solution.py:171
  270.4 3.4 %fusion.3 = bf16[1,256,2048]{2,1,0:T(8,128)(2,1)} fusion(f32[256,2048]{1,0:T(8,128)S(1)} %fusion.23, bf16[512,256]{1,0:T(8,128)(2,1)} %get-tuple-element.45, bf16[512,2048]{1,0:T(8,128)(2,1)} %get-tuple-element.46), kind=kOutput, calls=%fused_computation.6 | convolution fusion | flops 537919488 | bytes 5505024 | tf_op jit(solution)/shard_map/dot_general | solution.py:17
  274.6 7.3 %all-to-all-done.4 = bf16[64,32,128]{2,1,0:T(8,128)(2,1)S(1)} async-done(((bf16[64,32,128]{2,1,0:T(8,128)(2,1)}), bf16[64,32,128]{2,1,0:T(8,128)(2,1)S(1)}, u32[]{:S(2)}, u32[]{:S(2)}) %all-to-all-start.4) | async-done | bytes 524320 | tf_op jit(solution)/shard_map/all_to_all | solution.py:171
  285.1 3.5 %collective-permute-done.22 = f32[32,128]{1,0:T(8,128)S(1)} collective-permute-done((f32[32,128]{1,0:T(8,128)S(1)}, f32[32,128]{1,0:T(8,128)S(1)}, u32[]{:S(2)}, u32[]{:S(2)}) %collective-permute-start.22) | collective-permute-done | bytes 16416 | tf_op jit(solution)/shard_map/ppermute | solution.py:340
  (125 shorter events, 71.0 us)
Async XLA Ops:
  4.0 41.1 %all-to-all-start = ((bf16[64,16,512]{2,1,0:T(8,128)(2,1)}), bf16[64,16,512]{2,1,0:T(8,128)(2,1)S(1)}, u32[]{:S(2)}, u32[]{:S(2)}) async-start(bf16[64,16,512]{2,1,0:T(8,128)(2,1)} %bitcast.65), calls=%async_computation | async-start | bytes 2097152 | tf_op jit(solution)/shard_map/all_to_all | solution.py:171
  45.1 34.4 %all-to-all-start.1 = ((bf16[64,16,512]{2,1,0:T(8,128)(2,1)}), bf16[64,16,512]{2,1,0:T(8,128)(2,1)S(1)}, u32[]{:S(2)}, u32[]{:S(2)}) async-start(bf16[64,16,512]{2,1,0:T(8,128)(2,1)} %bitcast.50), calls=%async_computation.1 | async-start | bytes 2097152 | tf_op jit(solution)/shard_map/all_to_all | solution.py:171
  51.5 32.4 %collective-permute-start.1 = (bf16[512,512]{1,0:T(8,128)(2,1)S(1)}, bf16[512,512]{1,0:T(8,128)(2,1)}, u32[]{:S(2)}, u32[]{:S(2)}) collective-permute-start(bf16[512,512]{1,0:T(8,128)(2,1)S(1)} %bitcast.59), channel_id=1, source_target_pairs={{0,1},{1,2},{2,3},{3,0},{4,5},{5,6},{6,7},{7,4},{8,9},{9,10},{10,1... | collective-permute-start | bytes 1572872 | tf_op jit(solution)/shard_map/ppermute | solution.py:165
  52.9 31.5 %collective-permute-start = (bf16[512,512]{1,0:T(8,128)(2,1)S(1)}, bf16[512,512]{1,0:T(8,128)(2,1)}, u32[]{:S(2)}, u32[]{:S(2)}) collective-permute-start(bf16[512,512]{1,0:T(8,128)(2,1)S(1)} %bitcast.60), channel_id=1, source_target_pairs={{0,3},{1,0},{2,1},{3,2},{4,7},{5,4},{6,5},{7,6},{8,11},{9,8},{10,9... | collective-permute-start | bytes 1572872 | tf_op jit(solution)/shard_map/ppermute | solution.py:168
  79.7 13.9 %collective-permute-start.4 = (bf16[512,512]{1,0:T(8,128)(2,1)S(1)}, bf16[512,512]{1,0:T(8,128)(2,1)}, u32[]{:S(2)}, u32[]{:S(2)}) collective-permute-start(bf16[512,512]{1,0:T(8,128)(2,1)S(1)} %bitcast.62), channel_id=1, source_target_pairs={{0,1},{1,2},{2,3},{3,0},{4,5},{5,6},{6,7},{7,4},{8,9},{9,10},{10,1... | collective-permute-start | bytes 1572872 | tf_op jit(solution)/shard_map/ppermute | solution.py:165
  81.0 12.5 %collective-permute-start.3 = (bf16[512,512]{1,0:T(8,128)(2,1)S(1)}, bf16[512,512]{1,0:T(8,128)(2,1)S(1)}, u32[]{:S(2)}, u32[]{:S(2)}) collective-permute-start(bf16[512,512]{1,0:T(8,128)(2,1)S(1)} %bitcast.63), channel_id=1, source_target_pairs={{0,3},{1,0},{2,1},{3,2},{4,7},{5,4},{6,5},{7,6},{8,11},{9,8},{10,9... | collective-permute-start | bytes 1572872 | tf_op jit(solution)/shard_map/ppermute | solution.py:168
  82.6 21.8 %collective-permute-start.6 = (bf16[512,512]{1,0:T(8,128)(2,1)S(1)}, bf16[512,512]{1,0:T(8,128)(2,1)S(1)}, u32[]{:S(2)}, u32[]{:S(2)}) collective-permute-start(bf16[512,512]{1,0:T(8,128)(2,1)S(1)} %bitcast.56), channel_id=1, source_target_pairs={{0,3},{1,0},{2,1},{3,2},{4,7},{5,4},{6,5},{7,6},{8,11},{9,8},{10,9... | collective-permute-start | bytes 1572872 | tf_op jit(solution)/shard_map/ppermute | solution.py:168
  84.0 31.7 %collective-permute-start.9 = (bf16[512,512]{1,0:T(8,128)(2,1)S(1)}, bf16[512,512]{1,0:T(8,128)(2,1)S(1)}, u32[]{:S(2)}, u32[]{:S(2)}) collective-permute-start(bf16[512,512]{1,0:T(8,128)(2,1)S(1)} %bitcast.53), channel_id=1, source_target_pairs={{0,3},{1,0},{2,1},{3,2},{4,7},{5,4},{6,5},{7,6},{8,11},{9,8},{10,9... | collective-permute-start | bytes 1572872 | tf_op jit(solution)/shard_map/ppermute | solution.py:168
  84.4 32.6 %collective-permute-start.2 = (bf16[512,512]{1,0:T(8,128)(2,1)}, bf16[512,512]{1,0:T(8,128)(2,1)S(1)}, u32[]{:S(2)}, u32[]{:S(2)}) collective-permute-start(bf16[512,512]{1,0:T(8,128)(2,1)} %collective-permute-done.1.left), channel_id=1, source_target_pairs={{0,1},{1,2},{2,3},{3,0},{4,5},{5,6},{6,7},{7,4},{8,9},{9,10},{10,1... | collective-permute-start | bytes 1572872 | tf_op jit(solution)/shard_map/ppermute | solution.py:165
  93.5 31.5 %collective-permute-start.5 = (bf16[512,512]{1,0:T(8,128)(2,1)}, bf16[512,512]{1,0:T(8,128)(2,1)}, u32[]{:S(2)}, u32[]{:S(2)}) collective-permute-start(bf16[512,512]{1,0:T(8,128)(2,1)} %collective-permute-done.4.left), channel_id=1, source_target_pairs={{0,1},{1,2},{2,3},{3,0},{4,5},{5,6},{6,7},{7,4},{8,9},{9,10},{10,1... | collective-permute-start | bytes 1572872 | tf_op jit(solution)/shard_map/ppermute | solution.py:165
  93.5 41.6 %collective-permute-start.8 = (bf16[512,512]{1,0:T(8,128)(2,1)S(1)}, bf16[512,512]{1,0:T(8,128)(2,1)}, u32[]{:S(2)}, u32[]{:S(2)}) collective-permute-start(bf16[512,512]{1,0:T(8,128)(2,1)S(1)} %bitcast.57), channel_id=1, source_target_pairs={{0,1},{1,2},{2,3},{3,0},{4,5},{5,6},{6,7},{7,4},{8,9},{9,10},{10,1... | collective-permute-start | bytes 1572872 | tf_op jit(solution)/shard_map/ppermute | solution.py:165
  104.3 30.8 %collective-permute-start.7 = (bf16[512,512]{1,0:T(8,128)(2,1)S(1)}, bf16[512,512]{1,0:T(8,128)(2,1)}, u32[]{:S(2)}, u32[]{:S(2)}) collective-permute-start(bf16[512,512]{1,0:T(8,128)(2,1)S(1)} %collective-permute-done.6.right), channel_id=1, source_target_pairs={{0,3},{1,0},{2,1},{3,2},{4,7},{5,4},{6,5},{7,6},{8,11},{9,8},{10,9... | collective-permute-start | bytes 1572872 | tf_op jit(solution)/shard_map/ppermute | solution.py:168
  115.7 25.2 %collective-permute-start.11 = (bf16[512,512]{1,0:T(8,128)(2,1)S(1)}, bf16[512,512]{1,0:T(8,128)(2,1)}, u32[]{:S(2)}, u32[]{:S(2)}) collective-permute-start(bf16[512,512]{1,0:T(8,128)(2,1)S(1)} %bitcast.54), channel_id=1, source_target_pairs={{0,1},{1,2},{2,3},{3,0},{4,5},{5,6},{6,7},{7,4},{8,9},{9,10},{10,1... | collective-permute-start | bytes 1572872 | tf_op jit(solution)/shard_map/ppermute | solution.py:165
  117.8 23.1 %collective-permute-start.10 = (bf16[512,512]{1,0:T(8,128)(2,1)S(1)}, bf16[512,512]{1,0:T(8,128)(2,1)}, u32[]{:S(2)}, u32[]{:S(2)}) collective-permute-start(bf16[512,512]{1,0:T(8,128)(2,1)S(1)} %collective-permute-done.9.right), channel_id=1, source_target_pairs={{0,3},{1,0},{2,1},{3,2},{4,7},{5,4},{6,5},{7,6},{8,11},{9,8},{10,9... | collective-permute-start | bytes 1572872 | tf_op jit(solution)/shard_map/ppermute | solution.py:168
  135.0 20.0 %collective-permute-start.13 = (bf16[512,512]{1,0:T(8,128)(2,1)}, bf16[512,512]{1,0:T(8,128)(2,1)S(1)}, u32[]{:S(2)}, u32[]{:S(2)}) collective-permute-start(bf16[512,512]{1,0:T(8,128)(2,1)} %get-tuple-element.52), channel_id=1, source_target_pairs={{0,1},{1,2},{2,3},{3,0},{4,5},{5,6},{6,7},{7,4},{8,9},{9,10},{10,1... | collective-permute-start | bytes 1572872 | tf_op jit(solution)/shard_map/ppermute | solution.py:165
  150.8 9.6 %collective-permute-start.16 = (bf16[512,512]{1,0:T(8,128)(2,1)}, bf16[512,512]{1,0:T(8,128)(2,1)S(1)}, u32[]{:S(2)}, u32[]{:S(2)}) collective-permute-start(bf16[512,512]{1,0:T(8,128)(2,1)} %get-tuple-element.56), channel_id=1, source_target_pairs={{0,3},{1,0},{2,1},{3,2},{4,7},{5,4},{6,5},{7,6},{8,11},{9,8},{10,9... | collective-permute-start | bytes 1572872 | tf_op jit(solution)/shard_map/ppermute | solution.py:168
  153.5 18.1 %collective-permute-start.12 = (bf16[512,512]{1,0:T(8,128)(2,1)}, bf16[512,512]{1,0:T(8,128)(2,1)S(1)}, u32[]{:S(2)}, u32[]{:S(2)}) collective-permute-start(bf16[512,512]{1,0:T(8,128)(2,1)} %get-tuple-element.50), channel_id=1, source_target_pairs={{0,3},{1,0},{2,1},{3,2},{4,7},{5,4},{6,5},{7,6},{8,11},{9,8},{10,9... | collective-permute-start | bytes 1572872 | tf_op jit(solution)/shard_map/ppermute | solution.py:168
  153.8 17.9 %collective-permute-start.15 = (bf16[512,512]{1,0:T(8,128)(2,1)}, bf16[512,512]{1,0:T(8,128)(2,1)}, u32[]{:S(2)}, u32[]{:S(2)}) collective-permute-start(bf16[512,512]{1,0:T(8,128)(2,1)} %get-tuple-element.54), channel_id=1, source_target_pairs={{0,1},{1,2},{2,3},{3,0},{4,5},{5,6},{6,7},{7,4},{8,9},{9,10},{10,1... | collective-permute-start | bytes 1572872 | tf_op jit(solution)/shard_map/ppermute | solution.py:165
  155.2 19.6 %collective-permute-start.14 = (bf16[512,512]{1,0:T(8,128)(2,1)S(1)}, bf16[512,512]{1,0:T(8,128)(2,1)S(1)}, u32[]{:S(2)}, u32[]{:S(2)}) collective-permute-start(bf16[512,512]{1,0:T(8,128)(2,1)S(1)} %add_convert_fusion.1), channel_id=1, source_target_pairs={{0,1},{1,2},{2,3},{3,0},{4,5},{5,6},{6,7},{7,4},{8,9},{9,10},{10,1... | collective-permute-start | bytes 1572872 | tf_op jit(solution)/shard_map/ppermute | solution.py:165
  161.6 21.2 %collective-permute-start.17 = (bf16[512,512]{1,0:T(8,128)(2,1)S(1)}, bf16[512,512]{1,0:T(8,128)(2,1)S(1)}, u32[]{:S(2)}, u32[]{:S(2)}) collective-permute-start(bf16[512,512]{1,0:T(8,128)(2,1)S(1)} %add_convert_fusion), channel_id=1, source_target_pairs={{0,3},{1,0},{2,1},{3,2},{4,7},{5,4},{6,5},{7,6},{8,11},{9,8},{10,9... | collective-permute-start | bytes 1572872 | tf_op jit(solution)/shard_map/ppermute | solution.py:168
  164.9 22.7 %all-to-all-start.3 = ((bf16[4,512,128]{2,1,0:T(8,128)(2,1)}), bf16[4,512,128]{2,1,0:T(8,128)(2,1)S(1)}, u32[]{:S(2)}, u32[]{:S(2)}) async-start(bf16[4,512,128]{2,1,0:T(8,128)(2,1)} %bitcast.17), calls=%async_computation.3 | async-start | bytes 1048576 | tf_op jit(solution)/shard_map/all_to_all | solution.py:306
  188.4 42.9 %all-to-all-start.2 = ((bf16[64,16,512]{2,1,0:T(8,128)(2,1)}), bf16[64,16,512]{2,1,0:T(8,128)(2,1)S(1)}, u32[]{:S(2)}, u32[]{:S(2)}) async-start(bf16[64,16,512]{2,1,0:T(8,128)(2,1)} %bitcast.51), calls=%async_computation.2 | async-start | bytes 2097152 | tf_op jit(solution)/shard_map/all_to_all | solution.py:171
  235.6 12.5 %all-to-all-start.5 = ((f32[4,256,128]{2,1,0:T(8,128)}), f32[4,256,128]{2,1,0:T(8,128)S(1)}, u32[]{:S(2)}, u32[]{:S(2)}) async-start(f32[4,256,128]{2,1,0:T(8,128)} %get-tuple-element.58), calls=%async_computation.5 | async-start | bytes 1048576 | tf_op jit(solution)/shard_map/all_to_all | solution.py:342
  248.1 33.7 %all-to-all-start.4 = ((bf16[64,32,128]{2,1,0:T(8,128)(2,1)}), bf16[64,32,128]{2,1,0:T(8,128)(2,1)S(1)}, u32[]{:S(2)}, u32[]{:S(2)}) async-start(bf16[64,32,128]{2,1,0:T(8,128)(2,1)} %bitcast.21), calls=%async_computation.4 | async-start | bytes 1048576 | tf_op jit(solution)/shard_map/all_to_all | solution.py:171
  (36 other events, 545.8 us)

commit v2 on v1

v2 whole, which is shorter than its diff:
```python
import functools

import jax
import jax.numpy as jnp
from jax import lax
from jax.experimental import pallas as pl
from jax.experimental.pallas import tpu as pltpu
from jax.sharding import PartitionSpec as P


F32 = jnp.float32
BF16 = jnp.bfloat16
OVER_ROWS = (((0,), (0,)), ((), ()))
ACROSS = (((1,), (1,)), ((), ()))


def dot(a, b, dims=(((1,), (0,)), ((), ()))):
    return lax.dot_general(a, b, dims, preferred_element_type=F32)


def whole(shape):
    return pl.BlockSpec(shape, lambda *_: (0,) * len(shape))


def cost(flops, bytes_accessed):
    return pl.CostEstimate(flops=flops, bytes_accessed=bytes_accessed, transcendentals=0)


def find_slots(capacity, experts, ids_ref, dest_ref):
    tokens = ids_ref.shape[1]
    first, second = ids_ref[0:1, :], ids_ref[1:2, :]
    names = lax.broadcasted_iota(jnp.int32, (experts, tokens), 0)
    one = jnp.where(names == first, 1.0, 0.0)
    two = jnp.where(names == second, 1.0, 0.0)
    before = jnp.where(
        lax.broadcasted_iota(jnp.int32, (tokens, tokens), 0)
        < lax.broadcasted_iota(jnp.int32, (tokens, tokens), 1),
        1.0,
        0.0,
    ).astype(BF16)
    count_one = dot(one.astype(BF16), before)
    count_two = dot(two.astype(BF16), before) + jnp.sum(one, axis=1, keepdims=True)
    rank_one = jnp.sum(one * count_one, axis=0, keepdims=True).astype(jnp.int32)
    rank_two = jnp.sum(two * count_two, axis=0, keepdims=True).astype(jnp.int32)
    dest_ref[0:1, :] = first * capacity + rank_one
    dest_ref[1:2, :] = second * capacity + rank_two


def half_slots(rows, tokens, capacity, which):
    cut = capacity // 2
    index = lax.broadcasted_iota(jnp.int32, (rows, tokens), 0)
    return (index // cut) * capacity + lax.rem(index, cut) + which * cut


def fill_half(capacity, which, dest_ref, w_ref, x_ref, c_ref, out_ref):
    experts, cut = out_ref.shape[0], capacity // 2
    tokens, width = x_ref.shape
    slots = half_slots(experts * cut, tokens, capacity, which)
    one = jnp.where(slots == dest_ref[0:1, :], 1.0, 0.0)
    two = jnp.where(slots == dest_ref[1:2, :], 1.0, 0.0)
    hit = (one + two).astype(BF16)
    out_ref[:, 0] = dot(hit, x_ref[...]).reshape(experts, cut, width).astype(BF16)
    weight = jnp.sum(one * w_ref[0:1, :] + two * w_ref[1:2, :], axis=1, keepdims=True)
    rows = dot(hit, c_ref[...]) * weight
    out_ref[:, 1] = rows.reshape(experts, cut, width).astype(BF16)


def route_kernel(capacity, tp_ref, ids_ref, w_ref, x_ref, c_ref, dest_ref, out_ref):
    find_slots(capacity, out_ref.shape[0], ids_ref, dest_ref)
    fill_half(capacity, 0, dest_ref, w_ref, x_ref, c_ref, out_ref)


def rest_kernel(capacity, tp_ref, dest_ref, w_ref, x_ref, c_ref, out_ref):
    fill_half(capacity, 1, dest_ref, w_ref, x_ref, c_ref, out_ref)


def quarter(tp, by, n):
    return lax.rem(tp + by, n)


def up_kernel(n, tp_ref, own, right, opp, left, wg_ref, wu_ref, gate_ref, up_ref):
    tp = tp_ref[0]
    width = own.shape[1]
    gate = up = None
    for by, piece in enumerate((own, right, opp, left)):
        start = pl.multiple_of(quarter(tp, by, n) * width, width)
        x = piece[...]
        g = dot(x, wg_ref[pl.ds(start, width), :])
        u = dot(x, wu_ref[pl.ds(start, width), :])
        gate = g if gate is None else gate + g
        up = u if up is None else up + u
    gate_ref[...] = gate
    up_ref[...] = up


def down_kernel(
    n, tp_ref, own, right, opp, left, gate_ref, up_ref, wd_ref, wg_ref, wu_ref,
    hidden_ref, dgate_ref, dup_ref, own_out, right_out, opp_out, left_out,
):
    tp = tp_ref[0]
    width = own.shape[1]
    d_hidden = None
    for by, piece in enumerate((own, right, opp, left)):
        start = pl.multiple_of(quarter(tp, by, n) * width, width)
        d = dot(piece[...], wd_ref[:, pl.ds(start, width)], ACROSS)
        d_hidden = d if d_hidden is None else d_hidden + d
    gate, up = gate_ref[...], up_ref[...]
    sig = jax.nn.sigmoid(gate)
    silu = gate * sig
    hidden_ref[...] = (silu * up).astype(BF16)
    d_gate = (d_hidden * up * sig * (1.0 + gate * (1.0 - sig))).astype(BF16)
    d_up = (d_hidden * silu).astype(BF16)
    dgate_ref[...] = d_gate
    dup_ref[...] = d_up
    for by, out in enumerate((own_out, right_out, opp_out, left_out)):
        start = pl.multiple_of(quarter(tp, by, n) * width, width)
        rows = dot(d_gate, wg_ref[pl.ds(start, width), :], ACROSS)
        rows = rows + dot(d_up, wu_ref[pl.ds(start, width), :], ACROSS)
        out[...] = rows.astype(BF16)


def assemble_kernel(n, tp_ref, *refs):
    x_full, c_full, hidden, d_gate, d_up = refs[-5:]
    tp = tp_ref[0]
    width = refs[0].shape[1]
    for half in range(2):
        for by in range(n):
            start = pl.multiple_of(quarter(tp, by, n) * width, width)
            x_full[half, :, pl.ds(start, width)] = refs[n * half + by][...]
            c_full[half, :, pl.ds(start, width)] = refs[n * (2 + half) + by][...]
        for place, out in enumerate((hidden, d_gate, d_up)):
            out[half] = refs[4 * n + 3 * half + place][...]


def token_kernel(
    n, tp_ref, dest_ref, back_ref, cot_ref, p_own, p_right, p_opp, p_left,
    m_own, m_right, m_opp, m_left,
    grad_ref, mix_own, mix_right, mix_opp, mix_left,
):
    tp = tp_ref[0]
    tokens = dest_ref.shape[1]
    at = lax.broadcasted_iota(jnp.int32, (back_ref.shape[0], tokens), 0)
    hit = (at == dest_ref[0:1, :]) | (at == dest_ref[1:2, :])
    terms = dot(jnp.where(hit, 1.0, 0.0).astype(BF16), back_ref[...], OVER_ROWS)
    part = (cot_ref[...].astype(F32) + terms).astype(BF16)
    for by, piece in enumerate((m_own, m_right, m_opp, m_left)):
        g = dot(part, piece[...], OVER_ROWS).astype(BF16)
        grad_ref[:, quarter(tp, by, n)] = g.reshape(grad_ref.shape[0], *grad_ref.shape[2:])
    for piece, out in ((p_own, mix_own), (p_right, mix_right), (p_opp, mix_opp), (p_left, mix_left)):
        out[...] = dot(part, piece[...])


def shards(
    out_cotangent,
    stream,
    route_ids,
    route_weights,
    gate_proj,
    up_proj,
    down_proj,
    outer_gate,
    inner_gate,
    conv_input,
    conv_taps,
    out_proj,
):
    sp_devices = lax.axis_size("sp")
    n = lax.axis_size("tp")
    tp = lax.axis_index("tp").astype(jnp.int32)[None]
    tokens, width = stream.shape
    experts = sp_devices * gate_proj.shape[0]
    capacity = 4 * tokens // experts
    slots = experts * capacity
    q = width // n
    hidden_units = gate_proj.shape[2]
    channels = out_proj.shape[1]
    ahead = [(i, (i + 1) % n) for i in range(n)]
    back = [(i, (i - 1) % n) for i in range(n)]

    def to_right(x):
        return lax.ppermute(x, "tp", ahead)

    def to_left(x):
        return lax.ppermute(x, "tp", back)

    def over_sp(x):
        return lax.all_to_all(x, "sp", split_axis=0, concat_axis=0, tiled=True)

    ids = route_ids.T
    weights = route_weights.T
    cut = capacity // 2
    half = slots // 2
    mine = pl.BlockSpec((tokens, q), lambda i, t: (0, t[0]))
    pair = whole((2, tokens))
    packed = jax.ShapeDtypeStruct((experts, 2, cut, q), BF16)
    fill_cost = cost(4 * half * tokens * q, 8 * tokens * q)
    dest, send_a = pl.pallas_call(
        functools.partial(route_kernel, capacity),
        grid_spec=pltpu.PrefetchScalarGridSpec(
            num_scalar_prefetch=1,
            grid=(1,),
            in_specs=[pair, pair, mine, mine],
            out_specs=[pair, whole(packed.shape)],
        ),
        out_shape=[jax.ShapeDtypeStruct((2, tokens), jnp.int32), packed],
        cost_estimate=fill_cost,
        name="route",
    )(tp, ids, weights, stream, out_cotangent)
    send_b = pl.pallas_call(
        functools.partial(rest_kernel, capacity),
        grid_spec=pltpu.PrefetchScalarGridSpec(
            num_scalar_prefetch=1,
            grid=(1,),
            in_specs=[pair, pair, mine, mine],
            out_specs=whole(packed.shape),
        ),
        out_shape=packed,
        cost_estimate=fill_cost,
        name="rest",
    )(tp, dest, weights, stream, out_cotangent)
    got_a = over_sp(send_a.reshape(sp_devices, 2 * cut, q))
    got_b = over_sp(send_b.reshape(sp_devices, 2 * cut, q))

    def gathered(got):
        x = got[:, :cut].reshape(half, q)
        c = got[:, cut:].reshape(half, q)
        x_left = to_right(x)
        c_right = to_left(c)
        c_left = to_right(c)
        x_right = to_left(x)
        x_opp = to_right(x_left)
        c_opp = to_left(c_right)
        return (x, x_right, x_opp, x_left), (c, c_right, c_opp, c_left)

    w_gate, w_up, w_down = gate_proj[0], up_proj[0], down_proj[0]
    rows = 256
    piece = pl.BlockSpec((rows, q), lambda i, t: (i, 0))
    inner = pl.BlockSpec((rows, hidden_units), lambda i, t: (i, 0))

    def expert_up(pieces):
        return pl.pallas_call(
            functools.partial(up_kernel, n),
            grid_spec=pltpu.PrefetchScalarGridSpec(
                num_scalar_prefetch=1,
                grid=(half // rows,),
                in_specs=[piece] * 4 + [whole(w_gate.shape)] * 2,
                out_specs=[inner, inner],
            ),
            out_shape=[jax.ShapeDtypeStruct((half, hidden_units), F32)] * 2,
            cost_estimate=cost(4 * half * width * hidden_units, 4 * half * width),
            compiler_params=pltpu.CompilerParams(vmem_limit_bytes=20 << 20),
            name="expert_up",
        )(tp, *pieces, w_gate, w_up)

    def expert_down(pieces, gate, up):
        return pl.pallas_call(
            functools.partial(down_kernel, n),
            grid_spec=pltpu.PrefetchScalarGridSpec(
                num_scalar_prefetch=1,
                grid=(half // rows,),
                in_specs=[piece] * 4
                + [inner] * 2
                + [whole(w_down.shape), whole(w_gate.shape), whole(w_up.shape)],
                out_specs=[inner] * 3 + [piece] * 4,
            ),
            out_shape=[jax.ShapeDtypeStruct((half, hidden_units), BF16)] * 3
            + [jax.ShapeDtypeStruct((half, q), BF16)] * 4,
            cost_estimate=cost(6 * half * width * hidden_units, 6 * half * width),
            compiler_params=pltpu.CompilerParams(vmem_limit_bytes=30 << 20),
            name="expert_down",
        )(tp, *pieces, gate, up, w_down, w_gate, w_up)

    xa, ca = gathered(got_a)
    xb, cb = gathered(got_b)
    gate_a, up_a = expert_up(xa)
    gate_b, up_b = expert_up(xb)
    *inner_a, own_a, right_a, opp_a, left_a = expert_down(ca, gate_a, up_a)
    *inner_b, own_b, right_b, opp_b, left_b = expert_down(cb, gate_b, up_b)

    def added(*terms):
        total = terms[0].astype(F32)
        for term in terms[1:]:
            total = total + term.astype(F32)
        return total.astype(BF16)

    from_opp_a = to_right(opp_a)
    one_a = to_left(left_a)
    two_a = to_right(added(right_a, from_opp_a))
    from_opp_b = to_left(opp_b)
    one_b = to_right(right_b)
    two_b = to_left(added(left_b, from_opp_b))

    def returned_rows(own, one, two):
        return added(own, one, two).reshape(sp_devices, 1, cut, q)

    share = jnp.concatenate(
        [returned_rows(own_a, one_a, two_a), returned_rows(own_b, one_b, two_b)], axis=1
    )
    back_rows = over_sp(share.reshape(sp_devices, capacity, q)).reshape(slots, q)

    strips = 64
    piece = pl.BlockSpec((strips, q), lambda i, t: (i, 0))
    inner = pl.BlockSpec((strips, hidden_units), lambda i, t: (i, 0))
    outs = [(2, half, width)] * 2 + [(2, half, hidden_units)] * 3
    full = pl.pallas_call(
        functools.partial(assemble_kernel, n),
        grid_spec=pltpu.PrefetchScalarGridSpec(
            num_scalar_prefetch=1,
            grid=(half // strips,),
            in_specs=[piece] * (4 * n) + [inner] * 6,
            out_specs=[
                pl.BlockSpec((2, strips, shape[2]), lambda i, t: (0, i, 0)) for shape in outs
            ],
        ),
        out_shape=[jax.ShapeDtypeStruct(shape, BF16) for shape in outs],
        cost_estimate=cost(64 * slots * width, 8 * slots * width),
        name="assemble",
    )(tp, *xa, *xb, *ca, *cb, *inner_a, *inner_b)
    x_full, c_full, hidden, d_gate, d_up = [y.reshape(slots, y.shape[2]) for y in full]
    grad_gate = dot(x_full, d_gate, OVER_ROWS).astype(BF16)
    grad_up = dot(x_full, d_up, OVER_ROWS).astype(BF16)
    grad_down = dot(hidden, c_full, OVER_ROWS).astype(BF16)

    strip = width // sp_devices
    row_blocks = q // strip
    opposite = [(i, (i + 2) % n) for i in range(n)]

    def to_opposite(x):
        return lax.ppermute(x, "tp", opposite)

    mixed = inner_gate.astype(F32) * conv_input.astype(F32)
    sp_ahead = [(i, i + 1) for i in range(sp_devices - 1)]
    sp_back = [(i + 1, i) for i in range(sp_devices - 1)]
    previous = lax.ppermute(mixed[tokens - 2 :], "sp", sp_ahead)
    extended = jnp.concatenate([previous, mixed], axis=0)
    conv_out = (
        conv_taps[0] * extended[:tokens]
        + conv_taps[1] * extended[1 : tokens + 1]
        + conv_taps[2] * extended[2:]
    )
    mixer_out = (outer_gate.astype(F32) * conv_out).astype(BF16)
    mixer_left = to_right(mixer_out)
    mixer_right = to_left(mixer_out)
    mixer_opp = to_opposite(mixer_out)

    def block_of(by):
        return lax.dynamic_slice_in_dim(out_proj, lax.rem(tp[0] + by, n) * q, q, 0)

    proj_own = block_of(0)
    proj_left = to_right(block_of(1))
    proj_right = to_left(block_of(n - 1))
    proj_opp = to_opposite(block_of(2))

    partial_grad, mix_own, mix_right, mix_opp, mix_left = pl.pallas_call(
        functools.partial(token_kernel, n),
        grid_spec=pltpu.PrefetchScalarGridSpec(
            num_scalar_prefetch=1,
            grid=(1,),
            in_specs=[pair, whole((slots, q)), mine]
            + [whole((q, channels))] * 4
            + [whole((tokens, channels))] * 4,
            out_specs=[whole((row_blocks, n, strip, channels))] + [whole((tokens, channels))] * 4,
        ),
        out_shape=[jax.ShapeDtypeStruct((row_blocks, n, strip, channels), BF16)]
        + [jax.ShapeDtypeStruct((tokens, channels), F32)] * 4,
        cost_estimate=cost(2 * slots * tokens * q + 16 * tokens * q * channels, 4 * slots * q),
        compiler_params=pltpu.CompilerParams(vmem_limit_bytes=24 << 20),
        name="token",
    )(
        tp, dest, back_rows, out_cotangent,
        proj_own, proj_right, proj_opp, proj_left,
        mixer_out, mixer_right, mixer_opp, mixer_left,
    )
    pieces = over_sp(partial_grad.reshape(sp_devices, strip, channels))
    summed = pieces.astype(F32).sum(axis=0)
    home = [
        (s * n + t, (row_blocks * t + s // n) * n + s % n)
        for s in range(sp_devices)
        for t in range(n)
    ]
    grad_projection = lax.ppermute(summed, ("sp", "tp"), home)

    mix_from_left = to_right(mix_right)
    mix_from_right = to_left(mix_left)
    mix_from_opp = to_opposite(mix_opp)
    d_mixer = mix_own + mix_from_left + mix_from_right + mix_from_opp
    grad_outer = d_mixer * conv_out
    d_conv = d_mixer * outer_gate.astype(F32)
    following = lax.ppermute(d_conv[:2], "sp", sp_back)
    trailing = jnp.concatenate([d_conv, following], axis=0)
    d_mixed = (
        conv_taps[2] * trailing[:tokens]
        + conv_taps[1] * trailing[1 : tokens + 1]
        + conv_taps[0] * trailing[2:]
    )
    grad_inner = d_mixed * conv_input.astype(F32)
    grad_input = d_mixed * inner_gate.astype(F32)
    return (
        grad_gate[None],
        grad_up[None],
        grad_down[None],
        grad_projection,
        grad_outer,
        grad_inner,
        grad_input,
    )


def solution(mesh):
    placed = (
        P("sp", None),
        P("sp", None),
        P("sp", None),
        P("sp", None),
        P("sp", None, "tp"),
        P("sp", None, "tp"),
        P("sp", "tp", None),
        P("sp", "tp"),
        P("sp", "tp"),
        P("sp", "tp"),
        P(None, "tp"),
        P(None, "tp"),
    )
    return jax.shard_map(
        shards,
        mesh=mesh,
        in_specs=placed,
        out_specs=(
            P("sp", None, "tp"),
            P("sp", None, "tp"),
            P("sp", "tp", None),
            P("sp", "tp"),
            P("sp", "tp"),
            P("sp", "tp"),
            P("sp", "tp"),
        ),
        check_vma=False,
    )
```

time: 293 us -> 272 us (0.928)
  the two profiles are of different devices: /device:TPU:1 before, /device:TPU:51 now
where the time goes in v2:
time: 272 us; the launch traced here: 271 us
  waiting for transfers between devices  125 us (46%)
  starting transfers between devices  94.9 us (35%)
  Pallas kernels  28.4 us (10%)
  matrix products  11.7 us (4%)
  local copies, waits for them, and re-layouts  5.18 us (2%)
  other arithmetic  4.06 us (1%)
    all_to_all x4, starting transfers between devices, over_sp(): return lax.all_to_all(x, 'sp', split_axis=0, concat_axis=0, tiled=True)  60.3 us
    all_to_all x4, waiting for transfers between devices, over_sp(): return lax.all_to_all(x, 'sp', split_axis=0, concat_axis=0, tiled=True)  54.6 us
    ppermute x12, waiting for transfers between devices, to_right(): return lax.ppermute(x, 'tp', ahead)  40.9 us
    ppermute x12, waiting for transfers between devices, to_left(): return lax.ppermute(x, 'tp', back)  18.2 us
    ppermute x12, starting transfers between devices, to_right(): return lax.ppermute(x, 'tp', ahead)  16.5 us
    dot_general x3, matrix products, dot(): return lax.dot_general(a, b, dims, preferred_element_type=F32)  11.7 us
    ppermute x1, waiting for transfers between devices, shards(): grad_projection = lax.ppermute(summed, ('sp', 'tp'), home)  11 us
    pallas_call x1, Pallas kernels, shards(): pl.pallas_call(functools.partial(assemble_kernel, n), grid_spec=pltpu.Pre...  9.42 us
  transfers between devices with their start and end apart: 34, of which 16 were waited for; matrix products, arithmetic and copies ran while one was open for 6% of the time, Pallas kernels for 9%

profile of v2, /device:TPU:51, one launch (start us, length us, event | category | flops | bytes accessed | tf_op | source)
XLA Modules:
  0.0 270.9 jit_solution(17055347591968572681)
XLA Ops:
  0.6 2.7 %route.1 = (s32[2,256]{1,0:T(2,128)}, bf16[64,2,8,512]{3,2,1,0:T(8,128)(2,1)}) custom-call(s32[1]{0:T(128)} %bitcast.tp_ref, s32[2,256]{1,0:T(2,128)} %bitcast.75, f32[2,256]{1,0:T(2,128)} %bitcast.73, bf16[256,2048]{1,0:T(8,128)(2,1)} %x_ref.3, bf16[256,2048]{1,0:T(8,128)(2,1)} %cot_ref.1), custom_call_target="tpu_custom_call" | custom-call | flops 268435456 | bytes 1048576 | tf_op jit(solution)/shard_map/route/pallas_call | solution.py:197
  3.4 11.9 %all-to-all-start = ((bf16[64,16,512]{2,1,0:T(8,128)(2,1)}), bf16[64,16,512]{2,1,0:T(8,128)(2,1)S(1)}, u32[]{:S(2)}, u32[]{:S(2)}) async-start(bf16[64,16,512]{2,1,0:T(8,128)(2,1)} %bitcast.72), calls=%async_computation | async-start | bytes 2097152 | tf_op jit(solution)/shard_map/all_to_all | solution.py:187
  17.9 24.7 %all-to-all-done = bf16[64,16,512]{2,1,0:T(8,128)(2,1)S(1)} async-done(((bf16[64,16,512]{2,1,0:T(8,128)(2,1)}), bf16[64,16,512]{2,1,0:T(8,128)(2,1)S(1)}, u32[]{:S(2)}, u32[]{:S(2)}) %all-to-all-start) | async-done | bytes 1048608 | tf_op jit(solution)/shard_map/all_to_all | solution.py:187
  43.6 7.3 %all-to-all-start.1 = ((bf16[64,16,512]{2,1,0:T(8,128)(2,1)}), bf16[64,16,512]{2,1,0:T(8,128)(2,1)}, u32[]{:S(2)}, u32[]{:S(2)}) async-start(bf16[64,16,512]{2,1,0:T(8,128)(2,1)} %bitcast.71), calls=%async_computation.1 | async-start | bytes 2097152 | tf_op jit(solution)/shard_map/all_to_all | solution.py:187
  55.2 22.9 %all-to-all-done.1 = bf16[64,16,512]{2,1,0:T(8,128)(2,1)} async-done(((bf16[64,16,512]{2,1,0:T(8,128)(2,1)}), bf16[64,16,512]{2,1,0:T(8,128)(2,1)}, u32[]{:S(2)}, u32[]{:S(2)}) %all-to-all-start.1) | async-done | bytes 1048608 | tf_op jit(solution)/shard_map/all_to_all | solution.py:187
  82.8 9.2 %collective-permute-done.4.left.refs_7_ = bf16[512,512]{1,0:T(8,128)(2,1)S(1)} collective-permute-done((bf16[512,512]{1,0:T(8,128)(2,1)S(1)}, bf16[512,512]{1,0:T(8,128)(2,1)S(1)}, u32[]{:S(2)}, u32[]{:S(2)}) %collective-permute-start.4) | collective-permute-done | bytes 524320 | tf_op jit(solution)/shard_map/ppermute | solution.py:181
  94.4 8.9 %collective-permute-done.2.opp.refs_2_ = bf16[512,512]{1,0:T(8,128)(2,1)S(1)} collective-permute-done((bf16[512,512]{1,0:T(8,128)(2,1)}, bf16[512,512]{1,0:T(8,128)(2,1)S(1)}, u32[]{:S(2)}, u32[]{:S(2)}) %collective-permute-start.2) | collective-permute-done | bytes 524320 | tf_op jit(solution)/shard_map/ppermute | solution.py:181
  106.8 4.6 %expert_down.2 = (bf16[512,256]{1,0:T(8,128)(2,1)S(1)}, bf16[512,256]{1,0:T(8,128)(2,1)S(1)}, bf16[512,256]{1,0:T(8,128)(2,1)S(1)}, bf16[512,512]{1,0:T(8,128)(2...) custom-call(s32[1]{0:T(128)} %bitcast.tp_ref, ...), custom_call_target="tpu_custom_call" | custom-call | flops 1610612736 | bytes 6291456 | tf_op jit(solution)/shard_map/expert_down/pallas_call | solution.py:256
  116.8 9.0 %collective-permute-done.11.left.refs_15_ = bf16[512,512]{1,0:T(8,128)(2,1)S(1)} collective-permute-done((bf16[512,512]{1,0:T(8,128)(2,1)S(1)}, bf16[512,512]{1,0:T(8,128)(2,1)S(1)}, u32[]{:S(2)}, u32[]{:S(2)}) %collective-permute-start.11) | collective-permute-done | bytes 524320 | tf_op jit(solution)/shard_map/ppermute | solution.py:181
  126.5 3.3 %expert_down.3 = (bf16[512,256]{1,0:T(8,128)(2,1)S(1)}, bf16[512,256]{1,0:T(8,128)(2,1)S(1)}, bf16[512,256]{1,0:T(8,128)(2,1)S(1)}, bf16[512,512]{1,0:T(8,128)(2...) custom-call(s32[1]{0:T(128)} %bitcast.tp_ref, ...), custom_call_target="tpu_custom_call" | custom-call | flops 1610612736 | bytes 6291456 | tf_op jit(solution)/shard_map/expert_down/pallas_call | solution.py:256
  131.0 6.0 %collective-permute-done.13 = bf16[512,512]{1,0:T(8,128)(2,1)S(1)} collective-permute-done((bf16[512,512]{1,0:T(8,128)(2,1)S(1)}, bf16[512,512]{1,0:T(8,128)(2,1)S(1)}, u32[]{:S(2)}, u32[]{:S(2)}) %collective-permute-start.13) | collective-permute-done | bytes 524320 | tf_op jit(solution)/shard_map/ppermute | solution.py:181
  141.9 10.2 %collective-permute-done.12 = bf16[512,512]{1,0:T(8,128)(2,1)S(1)} collective-permute-done((bf16[512,512]{1,0:T(8,128)(2,1)S(1)}, bf16[512,512]{1,0:T(8,128)(2,1)S(1)}, u32[]{:S(2)}, u32[]{:S(2)}) %collective-permute-start.12) | collective-permute-done | bytes 524320 | tf_op jit(solution)/shard_map/ppermute | solution.py:184
  152.4 7.7 %collective-permute-done.15 = bf16[512,512]{1,0:T(8,128)(2,1)S(1)} collective-permute-done((bf16[512,512]{1,0:T(8,128)(2,1)S(1)}, bf16[512,512]{1,0:T(8,128)(2,1)S(1)}, u32[]{:S(2)}, u32[]{:S(2)}) %collective-permute-start.15) | collective-permute-done | bytes 524320 | tf_op jit(solution)/shard_map/ppermute | solution.py:181
  160.1 3.3 %collective-permute-done.17 = bf16[512,512]{1,0:T(8,128)(2,1)S(1)} collective-permute-done((bf16[512,512]{1,0:T(8,128)(2,1)S(1)}, bf16[512,512]{1,0:T(8,128)(2,1)S(1)}, u32[]{:S(2)}, u32[]{:S(2)}) %collective-permute-start.17) | collective-permute-done | bytes 524320 | tf_op jit(solution)/shard_map/ppermute | solution.py:184
  164.7 10.6 %all-to-all-start.2 = ((bf16[64,16,512]{2,1,0:T(8,128)(2,1)}), bf16[64,16,512]{2,1,0:T(8,128)(2,1)S(1)}, u32[]{:S(2)}, u32[]{:S(2)}) async-start(bf16[64,16,512]{2,1,0:T(8,128)(2,1)} %copy_bitcast_fusion), calls=%async_computation.2 | async-start | bytes 2097152 | tf_op jit(solution)/shard_map/all_to_all | solution.py:187
  175.4 3.4 %collective-permute-start.21 = (f32[2,128]{1,0:T(2,128)S(1)}, f32[2,128]{1,0:T(2,128)S(1)}, u32[]{:S(2)}, u32[]{:S(2)}) collective-permute-start(f32[2,128]{1,0:T(2,128)S(1)} %slice.59), channel_id=1, source_target_pairs={{0,4},{4,8},{8,12},{12,16},{16,20},{20,24},{24,28},{28,32},{32,36}... | collective-permute-start | bytes 3080 | tf_op jit(solution)/shard_map/ppermute | solution.py:334
  181.1 3.2 %collective-permute-start.19 = (bf16[512,128]{1,0:T(8,128)(2,1)S(1)}, bf16[512,128]{1,0:T(8,128)(2,1)S(1)}, u32[]{:S(2)}, u32[]{:S(2)}) collective-permute-start(bf16[512,128]{1,0:T(8,128)(2,1)S(1)} %get-tuple-element.80), channel_id=1, source_target_pairs={{0,2},{1,3},{2,0},{3,1},{4,6},{5,7},{6,4},{7,5},{8,10},{9,11},{10,... | collective-permute-start | bytes 393224 | tf_op jit(solution)/shard_map/ppermute | solution.py:329
  186.3 9.4 %assemble.1 = (bf16[2,512,2048]{2,1,0:T(8,128)(2,1)}, bf16[2,512,2048]{2,1,0:T(8,128)(2,1)}, bf16[2,512,256]{2,1,0:T(8,128)(2,1)}, bf16[2,512,256]{2,1,0:T(8,128)(2,1)}, bf16[2,512,256]{2,1,0:T(8,128)(2,1)}) custom-call(s32[1]{0:T(128)} %bitcast.tp_ref, bf16[512,512]{1,0:T(8,128)(2,1)} %copy-done.4, bf16[512,512]{1,0:T(8,128)(2,1)} %collective-permute-done.right.refs_1_, ...), custom_call_target="tpu_custom_call" | custom-call | flops 134217728 | bytes 16777216 | tf_op jit(solution)/shard_map/assemble/pallas_call | solution.py:305
  197.1 4.7 %fusion.4 = bf16[1,2048,256]{2,1,0:T(8,128)(2,1)} fusion(bf16[2,512,2048]{2,1,0:T(8,128)(2,1)} %get-tuple-element.49, bf16[2,512,256]{2,1,0:T(8,128)(2,1)} %get-tuple-element.51), kind=kOutput, calls=%fused_computation.7 | convolution fusion | flops 1074266112 | bytes 5767168 | tf_op jit(solution)/shard_map/dot_general | solution.py:18
  204.4 2.7 collective-permute-start.26
  208.9 30.6 %all-to-all-start.3 = ((bf16[64,32,128]{2,1,0:T(8,128)(2,1)}), bf16[64,32,128]{2,1,0:T(8,128)(2,1)S(1)}, u32[]{:S(2)}, u32[]{:S(2)}) async-start(bf16[64,32,128]{2,1,0:T(8,128)(2,1)} %bitcast.25), calls=%async_computation.3 | async-start | bytes 1048576 | tf_op jit(solution)/shard_map/all_to_all | solution.py:187
  239.5 4.8 %fusion.5 = bf16[1,2048,256]{2,1,0:T(8,128)(2,1)} fusion(bf16[2,512,2048]{2,1,0:T(8,128)(2,1)} %get-tuple-element.49, bf16[2,512,256]{2,1,0:T(8,128)(2,1)} %get-tuple-element.50), kind=kOutput, calls=%fused_computation.8 | convolution fusion | flops 1074266112 | bytes 5767168 | tf_op jit(solution)/shard_map/dot_general | solution.py:18
  250.3 6.2 %all-to-all-done.3 = bf16[64,32,128]{2,1,0:T(8,128)(2,1)S(1)} async-done(((bf16[64,32,128]{2,1,0:T(8,128)(2,1)}), bf16[64,32,128]{2,1,0:T(8,128)(2,1)S(1)}, u32[]{:S(2)}, u32[]{:S(2)}) %all-to-all-start.3) | async-done | bytes 524320 | tf_op jit(solution)/shard_map/all_to_all | solution.py:187
  259.3 11.0 %collective-permute-done.25 = f32[32,128]{1,0:T(8,128)S(1)} collective-permute-done((f32[32,128]{1,0:T(8,128)S(1)}, f32[32,128]{1,0:T(8,128)S(1)}, u32[]{:S(2)}, u32[]{:S(2)}) %collective-permute-start.25) | collective-permute-done | bytes 16416 | tf_op jit(solution)/shard_map/ppermute | solution.py:381
  (142 shorter events, 51.3 us)
Async XLA Ops:
  3.4 39.2 %all-to-all-start = ((bf16[64,16,512]{2,1,0:T(8,128)(2,1)}), bf16[64,16,512]{2,1,0:T(8,128)(2,1)S(1)}, u32[]{:S(2)}, u32[]{:S(2)}) async-start(bf16[64,16,512]{2,1,0:T(8,128)(2,1)} %bitcast.72), calls=%async_computation | async-start | bytes 2097152 | tf_op jit(solution)/shard_map/all_to_all | solution.py:187
  43.6 34.5 %all-to-all-start.1 = ((bf16[64,16,512]{2,1,0:T(8,128)(2,1)}), bf16[64,16,512]{2,1,0:T(8,128)(2,1)}, u32[]{:S(2)}, u32[]{:S(2)}) async-start(bf16[64,16,512]{2,1,0:T(8,128)(2,1)} %bitcast.71), calls=%async_computation.1 | async-start | bytes 2097152 | tf_op jit(solution)/shard_map/all_to_all | solution.py:187
  52.1 28.4 %collective-permute-start.1 = (bf16[512,512]{1,0:T(8,128)(2,1)S(1)}, bf16[512,512]{1,0:T(8,128)(2,1)}, u32[]{:S(2)}, u32[]{:S(2)}) collective-permute-start(bf16[512,512]{1,0:T(8,128)(2,1)S(1)} %get-tuple-element.76.own.refs_0_), channel_id=1, source_target_pairs={{0,1},{1,2},{2,3},{3,0},{4,5},{5,6},{6,7},{7,4},{8,9},{9,10},{10,1... | collective-permute-start | bytes 1572872 | tf_op jit(solution)/shard_map/ppermute | solution.py:181
  53.2 27.8 %collective-permute-start = (bf16[512,512]{1,0:T(8,128)(2,1)S(1)}, bf16[512,512]{1,0:T(8,128)(2,1)}, u32[]{:S(2)}, u32[]{:S(2)}) collective-permute-start(bf16[512,512]{1,0:T(8,128)(2,1)S(1)} %get-tuple-element.76.own.refs_0_), channel_id=1, source_target_pairs={{0,3},{1,0},{2,1},{3,2},{4,7},{5,4},{6,5},{7,6},{8,11},{9,8},{10,9... | collective-permute-start | bytes 1572872 | tf_op jit(solution)/shard_map/ppermute | solution.py:184
  53.7 28.3 %collective-permute-start.6 = (bf16[512,512]{1,0:T(8,128)(2,1)S(1)}, bf16[512,512]{1,0:T(8,128)(2,1)}, u32[]{:S(2)}, u32[]{:S(2)}) collective-permute-start(bf16[512,512]{1,0:T(8,128)(2,1)S(1)} %get-tuple-element.75.own.refs_8_), channel_id=1, source_target_pairs={{0,3},{1,0},{2,1},{3,2},{4,7},{5,4},{6,5},{7,6},{8,11},{9,8},{10,9... | collective-permute-start | bytes 1572872 | tf_op jit(solution)/shard_map/ppermute | solution.py:184
  53.9 28.7 %collective-permute-start.8 = (bf16[512,512]{1,0:T(8,128)(2,1)S(1)}, bf16[512,512]{1,0:T(8,128)(2,1)}, u32[]{:S(2)}, u32[]{:S(2)}) collective-permute-start(bf16[512,512]{1,0:T(8,128)(2,1)S(1)} %get-tuple-element.75.own.refs_8_), channel_id=1, source_target_pairs={{0,1},{1,2},{2,3},{3,0},{4,5},{5,6},{6,7},{7,4},{8,9},{9,10},{10,1... | collective-permute-start | bytes 1572872 | tf_op jit(solution)/shard_map/ppermute | solution.py:181
  81.0 22.3 %collective-permute-start.2 = (bf16[512,512]{1,0:T(8,128)(2,1)}, bf16[512,512]{1,0:T(8,128)(2,1)S(1)}, u32[]{:S(2)}, u32[]{:S(2)}) collective-permute-start(bf16[512,512]{1,0:T(8,128)(2,1)} %collective-permute-done.1.left.refs_3_), channel_id=1, source_target_pairs={{0,1},{1,2},{2,3},{3,0},{4,5},{5,6},{6,7},{7,4},{8,9},{9,10},{10,1... | collective-permute-start | bytes 1572872 | tf_op jit(solution)/shard_map/ppermute | solution.py:181
  82.0 24.7 %collective-permute-start.7 = (bf16[512,512]{1,0:T(8,128)(2,1)}, bf16[512,512]{1,0:T(8,128)(2,1)S(1)}, u32[]{:S(2)}, u32[]{:S(2)}) collective-permute-start(bf16[512,512]{1,0:T(8,128)(2,1)} %collective-permute-done.6.right.refs_9_), channel_id=1, source_target_pairs={{0,3},{1,0},{2,1},{3,2},{4,7},{5,4},{6,5},{7,6},{8,11},{9,8},{10,9... | collective-permute-start | bytes 1572872 | tf_op jit(solution)/shard_map/ppermute | solution.py:184
  82.5 32.8 %collective-permute-start.3 = (bf16[512,512]{1,0:T(8,128)(2,1)S(1)}, bf16[512,512]{1,0:T(8,128)(2,1)S(1)}, u32[]{:S(2)}, u32[]{:S(2)}) collective-permute-start(bf16[512,512]{1,0:T(8,128)(2,1)S(1)} %get-tuple-element.74.own.refs_4_), channel_id=1, source_target_pairs={{0,3},{1,0},{2,1},{3,2},{4,7},{5,4},{6,5},{7,6},{8,11},{9,8},{10,9... | collective-permute-start | bytes 1572872 | tf_op jit(solution)/shard_map/ppermute | solution.py:184
  92.1 23.2 %collective-permute-start.5 = (bf16[512,512]{1,0:T(8,128)(2,1)S(1)}, bf16[512,512]{1,0:T(8,128)(2,1)S(1)}, u32[]{:S(2)}, u32[]{:S(2)}) collective-permute-start(bf16[512,512]{1,0:T(8,128)(2,1)S(1)} %collective-permute-done.4.left.refs_7_), channel_id=1, source_target_pairs={{0,1},{1,2},{2,3},{3,0},{4,5},{5,6},{6,7},{7,4},{8,9},{9,10},{10,1... | collective-permute-start | bytes 1572872 | tf_op jit(solution)/shard_map/ppermute | solution.py:181
  93.1 32.7 %collective-permute-start.11 = (bf16[512,512]{1,0:T(8,128)(2,1)S(1)}, bf16[512,512]{1,0:T(8,128)(2,1)S(1)}, u32[]{:S(2)}, u32[]{:S(2)}) collective-permute-start(bf16[512,512]{1,0:T(8,128)(2,1)S(1)} %get-tuple-element.73.own.refs_12_), channel_id=1, source_target_pairs={{0,1},{1,2},{2,3},{3,0},{4,5},{5,6},{6,7},{7,4},{8,9},{9,10},{10,1... | collective-permute-start | bytes 1572872 | tf_op jit(solution)/shard_map/ppermute | solution.py:181
  103.3 23.2 %collective-permute-start.10 = (bf16[512,512]{1,0:T(8,128)(2,1)S(1)}, bf16[512,512]{1,0:T(8,128)(2,1)S(1)}, u32[]{:S(2)}, u32[]{:S(2)}) collective-permute-start(bf16[512,512]{1,0:T(8,128)(2,1)S(1)} %collective-permute-done.9.right.refs_13_), channel_id=1, source_target_pairs={{0,3},{1,0},{2,1},{3,2},{4,7},{5,4},{6,5},{7,6},{8,11},{9,8},{10,9... | collective-permute-start | bytes 1572872 | tf_op jit(solution)/shard_map/ppermute | solution.py:184
  111.4 25.6 %collective-permute-start.13 = (bf16[512,512]{1,0:T(8,128)(2,1)S(1)}, bf16[512,512]{1,0:T(8,128)(2,1)S(1)}, u32[]{:S(2)}, u32[]{:S(2)}) collective-permute-start(bf16[512,512]{1,0:T(8,128)(2,1)S(1)} %get-tuple-element.57), channel_id=1, source_target_pairs={{0,1},{1,2},{2,3},{3,0},{4,5},{5,6},{6,7},{7,4},{8,9},{9,10},{10,1... | collective-permute-start | bytes 1572872 | tf_op jit(solution)/shard_map/ppermute | solution.py:181
  130.5 21.7 %collective-permute-start.12 = (bf16[512,512]{1,0:T(8,128)(2,1)S(1)}, bf16[512,512]{1,0:T(8,128)(2,1)S(1)}, u32[]{:S(2)}, u32[]{:S(2)}) collective-permute-start(bf16[512,512]{1,0:T(8,128)(2,1)S(1)} %get-tuple-element.55), channel_id=1, source_target_pairs={{0,3},{1,0},{2,1},{3,2},{4,7},{5,4},{6,5},{7,6},{8,11},{9,8},{10,9... | collective-permute-start | bytes 1572872 | tf_op jit(solution)/shard_map/ppermute | solution.py:184
  138.2 21.9 %collective-permute-start.15 = (bf16[512,512]{1,0:T(8,128)(2,1)S(1)}, bf16[512,512]{1,0:T(8,128)(2,1)S(1)}, u32[]{:S(2)}, u32[]{:S(2)}) collective-permute-start(bf16[512,512]{1,0:T(8,128)(2,1)S(1)} %get-tuple-element.59), channel_id=1, source_target_pairs={{0,1},{1,2},{2,3},{3,0},{4,5},{5,6},{6,7},{7,4},{8,9},{9,10},{10,1... | collective-permute-start | bytes 1572872 | tf_op jit(solution)/shard_map/ppermute | solution.py:181
  141.1 22.3 %collective-permute-start.17 = (bf16[512,512]{1,0:T(8,128)(2,1)S(1)}, bf16[512,512]{1,0:T(8,128)(2,1)S(1)}, u32[]{:S(2)}, u32[]{:S(2)}) collective-permute-start(bf16[512,512]{1,0:T(8,128)(2,1)S(1)} %add_convert_fusion.1), channel_id=1, source_target_pairs={{0,3},{1,0},{2,1},{3,2},{4,7},{5,4},{6,5},{7,6},{8,11},{9,8},{10,9... | collective-permute-start | bytes 1572872 | tf_op jit(solution)/shard_map/ppermute | solution.py:184
  164.7 37.9 %all-to-all-start.2 = ((bf16[64,16,512]{2,1,0:T(8,128)(2,1)}), bf16[64,16,512]{2,1,0:T(8,128)(2,1)S(1)}, u32[]{:S(2)}, u32[]{:S(2)}) async-start(bf16[64,16,512]{2,1,0:T(8,128)(2,1)} %copy_bitcast_fusion), calls=%async_computation.2 | async-start | bytes 2097152 | tf_op jit(solution)/shard_map/all_to_all | solution.py:187
  179.9 21.8 %collective-permute-start.18 = (bf16[512,128]{1,0:T(8,128)(2,1)S(1)}, bf16[512,128]{1,0:T(8,128)(2,1)S(1)}, u32[]{:S(2)}, u32[]{:S(2)}) collective-permute-start(bf16[512,128]{1,0:T(8,128)(2,1)S(1)} %get-tuple-element.78), channel_id=1, source_target_pairs={{0,3},{1,0},{2,1},{3,2},{4,7},{5,4},{6,5},{7,6},{8,11},{9,8},{10,9... | collective-permute-start | bytes 393224 | tf_op jit(solution)/shard_map/ppermute | solution.py:184
  181.1 20.7 %collective-permute-start.19 = (bf16[512,128]{1,0:T(8,128)(2,1)S(1)}, bf16[512,128]{1,0:T(8,128)(2,1)S(1)}, u32[]{:S(2)}, u32[]{:S(2)}) collective-permute-start(bf16[512,128]{1,0:T(8,128)(2,1)S(1)} %get-tuple-element.80), channel_id=1, source_target_pairs={{0,2},{1,3},{2,0},{3,1},{4,6},{5,7},{6,4},{7,5},{8,10},{9,11},{10,... | collective-permute-start | bytes 393224 | tf_op jit(solution)/shard_map/ppermute | solution.py:329
  184.3 17.5 %collective-permute-start.20 = (bf16[512,128]{1,0:T(8,128)(2,1)S(1)}, bf16[512,128]{1,0:T(8,128)(2,1)S(1)}, u32[]{:S(2)}, u32[]{:S(2)}) collective-permute-start(bf16[512,128]{1,0:T(8,128)(2,1)S(1)} %get-tuple-element.77), channel_id=1, source_target_pairs={{0,1},{1,2},{2,3},{3,0},{4,5},{5,6},{6,7},{7,4},{8,9},{9,10},{10,1... | collective-permute-start | bytes 393224 | tf_op jit(solution)/shard_map/ppermute | solution.py:181
  204.4 39.8 %collective-permute-start.26 = (f32[256,128]{1,0:T(8,128)S(1)}, f32[256,128]{1,0:T(8,128)S(1)}, u32[]{:S(2)}, u32[]{:S(2)}) collective-permute-start(f32[256,128]{1,0:T(8,128)S(1)} %get-tuple-element.64), channel_id=1, source_target_pairs={{0,1},{1,2},{2,3},{3,0},{4,5},{5,6},{6,7},{7,4},{8,9},{9,10},{10,1... | collective-permute-start | bytes 393224 | tf_op jit(solution)/shard_map/ppermute | solution.py:181
  207.1 37.2 %collective-permute-start.27 = (f32[256,128]{1,0:T(8,128)S(1)}, f32[256,128]{1,0:T(8,128)S(1)}, u32[]{:S(2)}, u32[]{:S(2)}) collective-permute-start(f32[256,128]{1,0:T(8,128)S(1)} %get-tuple-element.65), channel_id=1, source_target_pairs={{0,3},{1,0},{2,1},{3,2},{4,7},{5,4},{6,5},{7,6},{8,11},{9,8},{10,9... | collective-permute-start | bytes 393224 | tf_op jit(solution)/shard_map/ppermute | solution.py:184
  207.1 37.2 %collective-permute-start.28 = (f32[256,128]{1,0:T(8,128)S(1)}, f32[256,128]{1,0:T(8,128)S(1)}, u32[]{:S(2)}, u32[]{:S(2)}) collective-permute-start(f32[256,128]{1,0:T(8,128)S(1)} %get-tuple-element.66), channel_id=1, source_target_pairs={{0,2},{1,3},{2,0},{3,1},{4,6},{5,7},{6,4},{7,5},{8,10},{9,11},{10,... | collective-permute-start | bytes 393224 | tf_op jit(solution)/shard_map/ppermute | solution.py:329
  208.9 47.6 %all-to-all-start.3 = ((bf16[64,32,128]{2,1,0:T(8,128)(2,1)}), bf16[64,32,128]{2,1,0:T(8,128)(2,1)S(1)}, u32[]{:S(2)}, u32[]{:S(2)}) async-start(bf16[64,32,128]{2,1,0:T(8,128)(2,1)} %bitcast.25), calls=%async_computation.3 | async-start | bytes 1048576 | tf_op jit(solution)/shard_map/all_to_all | solution.py:187
  (44 other events, 967.0 us)

commit v3 on v2

--- a/solution.py
+++ b/solution.py
@@ -93,25 +93,34 @@
     up_ref[...] = up
 
 
-def down_kernel(
-    n, tp_ref, own, right, opp, left, gate_ref, up_ref, wd_ref, wg_ref, wu_ref,
-    hidden_ref, dgate_ref, dup_ref, own_out, right_out, opp_out, left_out,
-):
-    tp = tp_ref[0]
-    width = own.shape[1]
+def activations(n, tp, pieces, gate_ref, up_ref, wd_ref, hidden_ref, dgate_ref, dup_ref):
+    width = pieces[0].shape[1]
     d_hidden = None
-    for by, piece in enumerate((own, right, opp, left)):
+    for by, piece in enumerate(pieces):
         start = pl.multiple_of(quarter(tp, by, n) * width, width)
         d = dot(piece[...], wd_ref[:, pl.ds(start, width)], ACROSS)
         d_hidden = d if d_hidden is None else d_hidden + d
     gate, up = gate_ref[...], up_ref[...]
     sig = jax.nn.sigmoid(gate)
     silu = gate * sig
-    hidden_ref[...] = (silu * up).astype(BF16)
+    hidden_ref[0] = (silu * up).astype(BF16)
     d_gate = (d_hidden * up * sig * (1.0 + gate * (1.0 - sig))).astype(BF16)
     d_up = (d_hidden * silu).astype(BF16)
-    dgate_ref[...] = d_gate
-    dup_ref[...] = d_up
+    dgate_ref[0] = d_gate
+    dup_ref[0] = d_up
+    return d_gate, d_up
+
+
+def down_kernel(
+    n, tp_ref, own, right, opp, left, gate_ref, up_ref, wd_ref, wg_ref, wu_ref,
+    first_hidden, first_dgate, first_dup,
+    hidden_ref, dgate_ref, dup_ref, own_out, right_out, opp_out, left_out,
+):
+    tp = tp_ref[0]
+    width = own.shape[1]
+    d_gate, d_up = activations(
+        n, tp, (own, right, opp, left), gate_ref, up_ref, wd_ref, hidden_ref, dgate_ref, dup_ref
+    )
     for by, out in enumerate((own_out, right_out, opp_out, left_out)):
         start = pl.multiple_of(quarter(tp, by, n) * width, width)
         rows = dot(d_gate, wg_ref[pl.ds(start, width), :], ACROSS)
@@ -119,8 +128,23 @@
         out[...] = rows.astype(BF16)
 
 
+def down_whole_kernel(
+    n, tp_ref, own, right, opp, left, gate_ref, up_ref, wd_ref, wg_ref, wu_ref,
+    hidden_ref, dgate_ref, dup_ref, rows_ref,
+):
+    width = own.shape[1]
+    d_gate, d_up = activations(
+        n, tp_ref[0], (own, right, opp, left), gate_ref, up_ref, wd_ref,
+        hidden_ref, dgate_ref, dup_ref,
+    )
+    for start in range(0, n * width, width):
+        rows = dot(d_gate, wg_ref[start : start + width, :], ACROSS)
+        rows = rows + dot(d_up, wu_ref[start : start + width, :], ACROSS)
+        rows_ref[:, start : start + width] = rows.astype(BF16)
+
+
 def assemble_kernel(n, tp_ref, *refs):
-    x_full, c_full, hidden, d_gate, d_up = refs[-5:]
+    x_full, c_full = refs[-2:]
     tp = tp_ref[0]
     width = refs[0].shape[1]
     for half in range(2):
@@ -128,26 +152,48 @@
             start = pl.multiple_of(quarter(tp, by, n) * width, width)
             x_full[half, :, pl.ds(start, width)] = refs[n * half + by][...]
             c_full[half, :, pl.ds(start, width)] = refs[n * (2 + half) + by][...]
-        for place, out in enumerate((hidden, d_gate, d_up)):
-            out[half] = refs[4 * n + 3 * half + place][...]
+
+
+def chosen_slots(capacity, which, rows, dest_ref):
+    at = half_slots(rows, dest_ref.shape[1], capacity, which)
+    hit = (at == dest_ref[0:1, :]) | (at == dest_ref[1:2, :])
+    return jnp.where(hit, 1.0, 0.0).astype(BF16)
+
+
+def fold_kernel(n, capacity, tp_ref, dest_ref, back_ref, own, right, opp, left):
+    tp = tp_ref[0]
+    width = own.shape[1]
+    hit = chosen_slots(capacity, 0, back_ref.shape[0], dest_ref)
+    for by, out in enumerate((own, right, opp, left)):
+        start = pl.multiple_of(quarter(tp, by, n) * width, width)
+        terms = dot(hit, back_ref[:, pl.ds(start, width)], OVER_ROWS)
+        out[...] = terms.astype(out.dtype)
 
 
 def token_kernel(
-    n, tp_ref, dest_ref, back_ref, cot_ref, p_own, p_right, p_opp, p_left,
-    m_own, m_right, m_opp, m_left,
-    grad_ref, mix_own, mix_right, mix_opp, mix_left,
+    capacity, tp_ref, dest_ref, back_ref, cot_ref, own, one, two, three,
+    p_own, p_right, p_opp, p_left, m_own, m_right, m_opp, m_left, *outs,
 ):
-    tp = tp_ref[0]
-    tokens = dest_ref.shape[1]
-    at = lax.broadcasted_iota(jnp.int32, (back_ref.shape[0], tokens), 0)
-    hit = (at == dest_ref[0:1, :]) | (at == dest_ref[1:2, :])
-    terms = dot(jnp.where(hit, 1.0, 0.0).astype(BF16), back_ref[...], OVER_ROWS)
+    hit = chosen_slots(capacity, 1, back_ref.shape[0], dest_ref)
+    terms = dot(hit, back_ref[...], OVER_ROWS) + own[...]
+    for other in (one, two, three):
+        terms = terms + other[...].astype(F32)
     part = (cot_ref[...].astype(F32) + terms).astype(BF16)
-    for by, piece in enumerate((m_own, m_right, m_opp, m_left)):
-        g = dot(part, piece[...], OVER_ROWS).astype(BF16)
-        grad_ref[:, quarter(tp, by, n)] = g.reshape(grad_ref.shape[0], *grad_ref.shape[2:])
-    for piece, out in ((p_own, mix_own), (p_right, mix_right), (p_opp, mix_opp), (p_left, mix_left)):
-        out[...] = dot(part, piece[...])
+    width = part.shape[1]
+    projs, mixers = (p_own, p_right, p_opp, p_left), (m_own, m_right, m_opp, m_left)
+    for proj, mixer, out in zip(projs, mixers, outs):
+        out[:width, :] = dot(part, mixer[...], OVER_ROWS).astype(BF16)
+        out[width:, :] = dot(part, proj[...]).astype(BF16)
+
+
+def place_kernel(n, tp_ref, own, right, opp, left, grad_ref, mix_ref):
+    width = grad_ref.shape[1]
+    total = None
+    for by, piece in enumerate((own, right, opp, left)):
+        grad_ref[quarter(tp_ref[0], by, n)] = piece[:width, :]
+        mix = piece[width:, :].astype(F32)
+        total = mix if total is None else total + mix
+    mix_ref[...] = total
 
 
 def shards(
@@ -252,30 +298,43 @@
             name="expert_up",
         )(tp, *pieces, w_gate, w_up)
 
-    def expert_down(pieces, gate, up):
+    def expert_down(kernel, which, out_specs, out_shape, pieces, gate, up, first):
+        kept = pl.BlockSpec((1, rows, hidden_units), lambda i, t: (which, i, 0))
         return pl.pallas_call(
-            functools.partial(down_kernel, n),
+            functools.partial(kernel, n),
             grid_spec=pltpu.PrefetchScalarGridSpec(
                 num_scalar_prefetch=1,
                 grid=(half // rows,),
                 in_specs=[piece] * 4
                 + [inner] * 2
-                + [whole(w_down.shape), whole(w_gate.shape), whole(w_up.shape)],
-                out_specs=[inner] * 3 + [piece] * 4,
+                + [whole(w_down.shape), whole(w_gate.shape), whole(w_up.shape)]
+                + [pl.BlockSpec(memory_space=pl.ANY)] * len(first),
+                out_specs=[kept] * 3 + out_specs,
             ),
-            out_shape=[jax.ShapeDtypeStruct((half, hidden_units), BF16)] * 3
-            + [jax.ShapeDtypeStruct((half, q), BF16)] * 4,
+            out_shape=[pltpu.HBM((2, half, hidden_units), BF16)] * 3 + out_shape,
+            input_output_aliases={10 + i: i for i in range(len(first))},
             cost_estimate=cost(6 * half * width * hidden_units, 6 * half * width),
             compiler_params=pltpu.CompilerParams(vmem_limit_bytes=30 << 20),
             name="expert_down",
-        )(tp, *pieces, gate, up, w_down, w_gate, w_up)
+        )(tp, *pieces, gate, up, w_down, w_gate, w_up, *first)
 
     xa, ca = gathered(got_a)
     xb, cb = gathered(got_b)
     gate_a, up_a = expert_up(xa)
     gate_b, up_b = expert_up(xb)
-    *inner_a, own_a, right_a, opp_a, left_a = expert_down(ca, gate_a, up_a)
-    *inner_b, own_b, right_b, opp_b, left_b = expert_down(cb, gate_b, up_b)
+    *inner_a, rows_a = expert_down(
+        down_whole_kernel,
+        0,
+        [pl.BlockSpec((rows, width), lambda i, t: (i, 0))],
+        [pltpu.HBM((half, width), BF16)],
+        ca, gate_a, up_a, (),
+    )
+    *inners, own_b, right_b, opp_b, left_b = expert_down(
+        down_kernel, 1, [piece] * 4, [jax.ShapeDtypeStruct((half, q), BF16)] * 4,
+        cb, gate_b, up_b, inner_a,
+    )
+
+    back_a = over_sp(rows_a.reshape(sp_devices, cut, width)).reshape(half, width)
 
     def added(*terms):
         total = terms[0].astype(F32)
@@ -283,51 +342,63 @@
             total = total + term.astype(F32)
         return total.astype(BF16)
 
-    from_opp_a = to_right(opp_a)
-    one_a = to_left(left_a)
-    two_a = to_right(added(right_a, from_opp_a))
+    opposite = [(i, (i + 2) % n) for i in range(n)]
+
+    def to_opposite(x):
+        return lax.ppermute(x, "tp", opposite)
+
+    def exchanged(right, opp, left):
+        from_left = to_right(right)
+        from_right = to_left(left)
+        from_opp = to_opposite(opp)
+        return from_right, from_opp, from_left
+
     from_opp_b = to_left(opp_b)
     one_b = to_right(right_b)
     two_b = to_left(added(left_b, from_opp_b))
-
-    def returned_rows(own, one, two):
-        return added(own, one, two).reshape(sp_devices, 1, cut, q)
-
-    share = jnp.concatenate(
-        [returned_rows(own_a, one_a, two_a), returned_rows(own_b, one_b, two_b)], axis=1
-    )
-    back_rows = over_sp(share.reshape(sp_devices, capacity, q)).reshape(slots, q)
+    share_b = added(own_b, one_b, two_b)
+    back_b = over_sp(share_b.reshape(sp_devices, cut, q)).reshape(half, q)
+    fold_own, *fold_rest = pl.pallas_call(
+        functools.partial(fold_kernel, n, capacity),
+        grid_spec=pltpu.PrefetchScalarGridSpec(
+            num_scalar_prefetch=1,
+            grid=(1,),
+            in_specs=[pair, whole((half, width))],
+            out_specs=[whole((tokens, q))] * 4,
+        ),
+        out_shape=[jax.ShapeDtypeStruct((tokens, q), F32)]
+        + [jax.ShapeDtypeStruct((tokens, q), BF16)] * 3,
+        cost_estimate=cost(2 * half * tokens * width, 2 * half * width),
+        compiler_params=pltpu.CompilerParams(vmem_limit_bytes=24 << 20),
+        name="fold",
+    )(tp, dest, back_a)
+    fold_others = exchanged(*fold_rest)
 
     strips = 64
     piece = pl.BlockSpec((strips, q), lambda i, t: (i, 0))
-    inner = pl.BlockSpec((strips, hidden_units), lambda i, t: (i, 0))
-    outs = [(2, half, width)] * 2 + [(2, half, hidden_units)] * 3
+    outs = [(2, half, width)] * 2
     full = pl.pallas_call(
         functools.partial(assemble_kernel, n),
         grid_spec=pltpu.PrefetchScalarGridSpec(
             num_scalar_prefetch=1,
             grid=(half // strips,),
-            in_specs=[piece] * (4 * n) + [inner] * 6,
+            in_specs=[piece] * (4 * n),
             out_specs=[
                 pl.BlockSpec((2, strips, shape[2]), lambda i, t: (0, i, 0)) for shape in outs
             ],
         ),
-        out_shape=[jax.ShapeDtypeStruct(shape, BF16) for shape in outs],
+        out_shape=[pltpu.HBM(shape, BF16) for shape in outs],
         cost_estimate=cost(64 * slots * width, 8 * slots * width),
+        compiler_params=pltpu.CompilerParams(vmem_limit_bytes=20 << 20),
         name="assemble",
-    )(tp, *xa, *xb, *ca, *cb, *inner_a, *inner_b)
-    x_full, c_full, hidden, d_gate, d_up = [y.reshape(slots, y.shape[2]) for y in full]
+    )(tp, *xa, *xb, *ca, *cb)
+    x_full, c_full = [y.reshape(slots, width) for y in full]
+    hidden, d_gate, d_up = [y.reshape(slots, hidden_units) for y in inners]
     grad_gate = dot(x_full, d_gate, OVER_ROWS).astype(BF16)
     grad_up = dot(x_full, d_up, OVER_ROWS).astype(BF16)
     grad_down = dot(hidden, c_full, OVER_ROWS).astype(BF16)
 
     strip = width // sp_devices
-    row_blocks = q // strip
-    opposite = [(i, (i + 2) % n) for i in range(n)]
-
-    def to_opposite(x):
-        return lax.ppermute(x, "tp", opposite)
-
     mixed = inner_gate.astype(F32) * conv_input.astype(F32)
     sp_ahead = [(i, i + 1) for i in range(sp_devices - 1)]
     sp_back = [(i + 1, i) for i in range(sp_devices - 1)]
@@ -351,39 +422,47 @@
     proj_right = to_left(block_of(n - 1))
     proj_opp = to_opposite(block_of(2))
 
-    partial_grad, mix_own, mix_right, mix_opp, mix_left = pl.pallas_call(
-        functools.partial(token_kernel, n),
+    packed_block = (q + tokens, channels)
+    own_block, *other_blocks = pl.pallas_call(
+        functools.partial(token_kernel, capacity),
         grid_spec=pltpu.PrefetchScalarGridSpec(
             num_scalar_prefetch=1,
             grid=(1,),
-            in_specs=[pair, whole((slots, q)), mine]
+            in_specs=[pair, whole((half, q)), mine]
+            + [whole((tokens, q))] * 4
             + [whole((q, channels))] * 4
             + [whole((tokens, channels))] * 4,
-            out_specs=[whole((row_blocks, n, strip, channels))] + [whole((tokens, channels))] * 4,
-        ),
-        out_shape=[jax.ShapeDtypeStruct((row_blocks, n, strip, channels), BF16)]
-        + [jax.ShapeDtypeStruct((tokens, channels), F32)] * 4,
+            out_specs=[whole(packed_block)] * n,
+        ),
+        out_shape=[jax.ShapeDtypeStruct(packed_block, BF16)] * n,
         cost_estimate=cost(2 * slots * tokens * q + 16 * tokens * q * channels, 4 * slots * q),
         compiler_params=pltpu.CompilerParams(vmem_limit_bytes=24 << 20),
         name="token",
     )(
-        tp, dest, back_rows, out_cotangent,
+        tp, dest, back_b, out_cotangent, fold_own, *fold_others,
         proj_own, proj_right, proj_opp, proj_left,
         mixer_out, mixer_right, mixer_opp, mixer_left,
     )
+    other_blocks = exchanged(*other_blocks)
+    partial_grad, d_mixer = pl.pallas_call(
+        functools.partial(place_kernel, n),
+        grid_spec=pltpu.PrefetchScalarGridSpec(
+            num_scalar_prefetch=1,
+            grid=(1,),
+            in_specs=[whole(packed_block)] * 4,
+            out_specs=[whole((n, q, channels)), whole((tokens, channels))],
+        ),
+        out_shape=[
+            pltpu.HBM((n, q, channels), BF16),
+            jax.ShapeDtypeStruct((tokens, channels), F32),
+        ],
+        cost_estimate=cost(4 * tokens * channels, 4 * width * channels),
+        compiler_params=pltpu.CompilerParams(vmem_limit_bytes=24 << 20),
+        name="place",
+    )(tp, own_block, *other_blocks)
     pieces = over_sp(partial_grad.reshape(sp_devices, strip, channels))
-    summed = pieces.astype(F32).sum(axis=0)
-    home = [
-        (s * n + t, (row_blocks * t + s // n) * n + s % n)
-        for s in range(sp_devices)
-        for t in range(n)
-    ]
-    grad_projection = lax.ppermute(summed, ("sp", "tp"), home)
-
-    mix_from_left = to_right(mix_right)
-    mix_from_right = to_left(mix_left)
-    mix_from_opp = to_opposite(mix_opp)
-    d_mixer = mix_own + mix_from_left + mix_from_right + mix_from_opp
+    grad_projection = pieces.astype(F32).sum(axis=0)
+
     grad_outer = d_mixer * conv_out
     d_conv = d_mixer * outer_gate.astype(F32)
     following = lax.ppermute(d_conv[:2], "sp", sp_back)

time: 272 us -> 298 us (1.096)
  the two profiles are of different devices: /device:TPU:51 before, /device:TPU:1 now
where the time goes in v3:
time: 298 us; the launch traced here: 297 us
  waiting for transfers between devices  130 us (44%)
  starting transfers between devices  94 us (32%)
  Pallas kernels  27.6 us (9%)
  local copies, waits for them, and re-layouts  22.5 us (8%)
  matrix products  13.7 us (5%)
  other arithmetic  7.66 us (3%)
    all_to_all x5, starting transfers between devices, over_sp(): return lax.all_to_all(x, 'sp', split_axis=0, concat_axis=0, tiled=True)  61.1 us
    ppermute x11, waiting for transfers between devices, to_right(): return lax.ppermute(x, 'tp', ahead)  56.9 us
    ppermute x12, waiting for transfers between devices, to_left(): return lax.ppermute(x, 'tp', back)  37.1 us
    all_to_all x5, waiting for transfers between devices, over_sp(): return lax.all_to_all(x, 'sp', split_axis=0, concat_axis=0, tiled=True)  34.3 us
    unnamed x108, local copies, waits for them, and re-layouts  17.9 us
    ppermute x12, starting transfers between devices, to_left(): return lax.ppermute(x, 'tp', back)  17.1 us
    dot_general x3, matrix products, dot(): return lax.dot_general(a, b, dims, preferred_element_type=F32)  13.7 us
    pallas_call x2, Pallas kernels, expert_down(): pl.pallas_call(functools.partial(kernel, n), grid_spec=pltpu.PrefetchScal...  8.41 us
  transfers between devices with their start and end apart: 34, of which 17 were waited for; matrix products, arithmetic and copies ran while one was open for 9% of the time, Pallas kernels for 7%

profile of v3, /device:TPU:1, one launch (start us, length us, event | category | flops | bytes accessed | tf_op | source)
XLA Modules:
  0.0 296.6 jit_solution(362538941772720825)
XLA Ops:
  3.4 13.0 %all-to-all-start = ((bf16[64,16,512]{2,1,0:T(8,128)(2,1)}), bf16[64,16,512]{2,1,0:T(8,128)(2,1)S(1)}, u32[]{:S(2)}, u32[]{:S(2)}) async-start(bf16[64,16,512]{2,1,0:T(8,128)(2,1)} %bitcast.70), calls=%async_computation | async-start | bytes 2097152 | tf_op jit(solution)/shard_map/all_to_all | solution.py:233
  19.0 25.5 %all-to-all-done = bf16[64,16,512]{2,1,0:T(8,128)(2,1)S(1)} async-done(((bf16[64,16,512]{2,1,0:T(8,128)(2,1)}), bf16[64,16,512]{2,1,0:T(8,128)(2,1)S(1)}, u32[]{:S(2)}, u32[]{:S(2)}) %all-to-all-start) | async-done | bytes 1048608 | tf_op jit(solution)/shard_map/all_to_all | solution.py:233
  45.5 6.5 %all-to-all-start.1 = ((bf16[64,16,512]{2,1,0:T(8,128)(2,1)}), bf16[64,16,512]{2,1,0:T(8,128)(2,1)}, u32[]{:S(2)}, u32[]{:S(2)}) async-start(bf16[64,16,512]{2,1,0:T(8,128)(2,1)} %bitcast.68), calls=%async_computation.1 | async-start | bytes 2097152 | tf_op jit(solution)/shard_map/all_to_all | solution.py:233
  57.6 10.2 %collective-permute-done.1.refs_3_.left = bf16[512,512]{1,0:T(8,128)(2,1)S(1)} collective-permute-done((bf16[512,512]{1,0:T(8,128)(2,1)S(1)}, bf16[512,512]{1,0:T(8,128)(2,1)S(1)}, u32[]{:S(2)}, u32[]{:S(2)}) %collective-permute-start.1) | collective-permute-done | bytes 524320 | tf_op jit(solution)/shard_map/ppermute | solution.py:227
  70.6 8.1 %collective-permute-done.refs_1_.right = bf16[512,512]{1,0:T(8,128)(2,1)S(1)} collective-permute-done((bf16[512,512]{1,0:T(8,128)(2,1)S(1)}, bf16[512,512]{1,0:T(8,128)(2,1)S(1)}, u32[]{:S(2)}, u32[]{:S(2)}) %collective-permute-start) | collective-permute-done | bytes 524320 | tf_op jit(solution)/shard_map/ppermute | solution.py:230
  82.8 9.8 %collective-permute-done.8.refs_11_.left = bf16[512,512]{1,0:T(8,128)(2,1)S(1)} collective-permute-done((bf16[512,512]{1,0:T(8,128)(2,1)S(1)}, bf16[512,512]{1,0:T(8,128)(2,1)S(1)}, u32[]{:S(2)}, u32[]{:S(2)}) %collective-permute-start.8) | collective-permute-done | bytes 524320 | tf_op jit(solution)/shard_map/ppermute | solution.py:227
  92.6 4.3 %expert_down.2 = (bf16[2,512,256]{2,1,0:T(8,128)(2,1)}, bf16[2,512,256]{2,1,0:T(8,128)(2,1)}, bf16[2,512,256]{2,1,0:T(8,128)(2,1)}, bf16[512,2048]{1,0:T(8,128)(2,1)}) custom-call(s32[1]{0:T(128)} %bitcast.tp_ref, bf16[512,512]{1,0:T(8,128)(2,1)S(1)} %get-tuple-element.71.refs_8_.own, bf16[512,512]{1,0:T(8,128)(2,1)S(1)} %collective-permute-done.6.refs_9_.right, ...), custom_call_target="tpu_custom_call" | custom-call | flops 1610612736 | bytes 6291456 | tf_op jit(solution)/shard_map/expert_down/pallas_call | solution.py:303
  98.5 12.3 %all-to-all-start.3 = ((bf16[64,8,2048]{2,1,0:T(8,128)(2,1)}), bf16[64,8,2048]{2,1,0:T(8,128)(2,1)}, u32[]{:S(2)}, u32[]{:S(2)}) async-start(bf16[64,8,2048]{2,1,0:T(8,128)(2,1)} %bitcast.69), calls=%async_computation.3 | async-start | bytes 4194304 | tf_op jit(solution)/shard_map/all_to_all | solution.py:233
  115.0 11.6 %collective-permute-done.4.refs_7_.left = bf16[512,512]{1,0:T(8,128)(2,1)S(1)} collective-permute-done((bf16[512,512]{1,0:T(8,128)(2,1)S(1)}, bf16[512,512]{1,0:T(8,128)(2,1)S(1)}, u32[]{:S(2)}, u32[]{:S(2)}) %collective-permute-start.4) | collective-permute-done | bytes 524320 | tf_op jit(solution)/shard_map/ppermute | solution.py:227
  129.4 7.3 %collective-permute-done.3.refs_5_.right = bf16[512,512]{1,0:T(8,128)(2,1)S(1)} collective-permute-done((bf16[512,512]{1,0:T(8,128)(2,1)S(1)}, bf16[512,512]{1,0:T(8,128)(2,1)S(1)}, u32[]{:S(2)}, u32[]{:S(2)}) %collective-permute-start.3) | collective-permute-done | bytes 524320 | tf_op jit(solution)/shard_map/ppermute | solution.py:230
  141.6 9.8 %collective-permute-done.11.refs_15_.left = bf16[512,512]{1,0:T(8,128)(2,1)S(1)} collective-permute-done((bf16[512,512]{1,0:T(8,128)(2,1)S(1)}, bf16[512,512]{1,0:T(8,128)(2,1)S(1)}, u32[]{:S(2)}, u32[]{:S(2)}) %collective-permute-start.11) | collective-permute-done | bytes 524320 | tf_op jit(solution)/shard_map/ppermute | solution.py:227
  151.4 4.1 %expert_down.3 = (bf16[2,512,256]{2,1,0:T(8,128)(2,1)}, bf16[2,512,256]{2,1,0:T(8,128)(2,1)}, bf16[2,512,256]{2,1,0:T(8,128)(2,1)}, bf16[512,512]{1,0:T(8,128)(2...) custom-call(s32[1]{0:T(128)} %bitcast.tp_ref, ...), custom_call_target="tpu_custom_call", output_to_operand_aliasing={{0}: (10, {}), {1}: (11, {}), {2}: (12, {})} | custom-call | flops 1610612736 | bytes 6291456 | tf_op jit(solution)/shard_map/expert_down/pallas_call | solution.py:303
  157.1 10.1 %collective-permute-done.13 = bf16[512,512]{1,0:T(8,128)(2,1)S(1)} collective-permute-done((bf16[512,512]{1,0:T(8,128)(2,1)S(1)}, bf16[512,512]{1,0:T(8,128)(2,1)S(1)}, u32[]{:S(2)}, u32[]{:S(2)}) %collective-permute-start.13) | collective-permute-done | bytes 524320 | tf_op jit(solution)/shard_map/ppermute | solution.py:230
  171.6 7.6 %collective-permute-done.14 = bf16[512,512]{1,0:T(8,128)(2,1)} collective-permute-done((bf16[512,512]{1,0:T(8,128)(2,1)}, bf16[512,512]{1,0:T(8,128)(2,1)}, u32[]{:S(2)}, u32[]{:S(2)}) %collective-permute-start.14) | collective-permute-done | bytes 524320 | tf_op jit(solution)/shard_map/ppermute | solution.py:230
  181.6 15.4 %all-to-all-start.2 = ((bf16[64,8,512]{2,1,0:T(8,128)(2,1)}), bf16[64,8,512]{2,1,0:T(8,128)(2,1)}, u32[]{:S(2)}, u32[]{:S(2)}) async-start(bf16[64,8,512]{2,1,0:T(8,128)(2,1)} %fusion.6), calls=%async_computation.2 | async-start | bytes 1048576 | tf_op jit(solution)/shard_map/all_to_all | solution.py:233
  218.9 4.8 %assemble.1 = (bf16[2,512,2048]{2,1,0:T(8,128)(2,1)}, bf16[2,512,2048]{2,1,0:T(8,128)(2,1)}) custom-call(s32[1]{0:T(128)} %bitcast.tp_ref, bf16[512,512]{1,0:T(8,128)(2,1)S(1)} %get-tuple-element.72.refs_0_.own, bf16[512,512]{1,0:T(8,128)(2,1)S(1)} %copy-done.14, bf16[512,512]{1,0:T(8,128)(2,1)S(1)} %copy-done.16, bf16[512,512]{1,0:T(8,128)(2,1)S(1)} %copy-done.10, ...), custom_call_target="tpu_custom_call" | custom-call | flops 134217728 | bytes 16777216 | tf_op jit(solution)/shard_map/assemble/pallas_call | solution.py:380
  230.8 4.6 %fusion.4 = bf16[1,2048,256]{2,1,0:T(8,128)(2,1)} fusion(bf16[2,512,2048]{2,1,0:T(8,128)(2,1)} %get-tuple-element.38, bf16[2,512,256]{2,1,0:T(8,128)(2,1)S(1)} %copy-done.45), kind=kOutput, calls=%fused_computation.7 | convolution fusion | flops 1074266112 | bytes 5767168 | tf_op jit(solution)/shard_map/dot_general | solution.py:18
  236.8 4.0 %collective-permute-done.15.one = bf16[256,512]{1,0:T(8,128)(2,1)S(1)} collective-permute-done((bf16[256,512]{1,0:T(8,128)(2,1)}, bf16[256,512]{1,0:T(8,128)(2,1)S(1)}, u32[]{:S(2)}, u32[]{:S(2)}) %collective-permute-start.15) | collective-permute-done | bytes 262176 | tf_op jit(solution)/shard_map/ppermute | solution.py:230
  240.8 4.0 %collective-permute-done.17.three = bf16[256,512]{1,0:T(8,128)(2,1)S(1)} collective-permute-done((bf16[256,512]{1,0:T(8,128)(2,1)S(1)}, bf16[256,512]{1,0:T(8,128)(2,1)S(1)}, u32[]{:S(2)}, u32[]{:S(2)}) %collective-permute-start.17) | collective-permute-done | bytes 262176 | tf_op jit(solution)/shard_map/ppermute | solution.py:227
  252.1 4.7 %fusion.5 = bf16[1,2048,256]{2,1,0:T(8,128)(2,1)} fusion(bf16[2,512,2048]{2,1,0:T(8,128)(2,1)} %get-tuple-element.38, bf16[2,512,256]{2,1,0:T(8,128)(2,1)} %get-tuple-element.46), kind=kOutput, calls=%fused_computation.8 | convolution fusion | flops 1074266112 | bytes 5767168 | tf_op jit(solution)/shard_map/dot_general | solution.py:18
  257.8 5.6 %collective-permute-done.27.left = bf16[768,128]{1,0:T(8,128)(2,1)S(1)} collective-permute-done((bf16[768,128]{1,0:T(8,128)(2,1)S(1)}, bf16[768,128]{1,0:T(8,128)(2,1)S(1)}, u32[]{:S(2)}, u32[]{:S(2)}) %collective-permute-start.27) | collective-permute-done | bytes 196640 | tf_op jit(solution)/shard_map/ppermute | solution.py:227
  264.3 13.9 %all-to-all-start.4 = ((bf16[64,32,128]{2,1,0:T(8,128)(2,1)}), bf16[64,32,128]{2,1,0:T(8,128)(2,1)S(1)}, u32[]{:S(2)}, u32[]{:S(2)}) async-start(bf16[64,32,128]{2,1,0:T(8,128)(2,1)} %bitcast.71), calls=%async_computation.4 | async-start | bytes 1048576 | tf_op jit(solution)/shard_map/all_to_all | solution.py:233
  281.3 4.4 %fusion.3 = bf16[1,256,2048]{2,1,0:T(8,128)(2,1)} fusion(bf16[2,512,256]{2,1,0:T(8,128)(2,1)S(1)} %copy-done.44, bf16[2,512,2048]{2,1,0:T(8,128)(2,1)} %get-tuple-element.49), kind=kOutput, calls=%fused_computation.6 | convolution fusion | flops 1074266112 | bytes 5767168 | tf_op jit(solution)/shard_map/dot_general | solution.py:18
  287.1 8.8 %all-to-all-done.4 = bf16[64,32,128]{2,1,0:T(8,128)(2,1)S(1)} async-done(((bf16[64,32,128]{2,1,0:T(8,128)(2,1)}), bf16[64,32,128]{2,1,0:T(8,128)(2,1)S(1)}, u32[]{:S(2)}, u32[]{:S(2)}) %all-to-all-start.4) | async-done | bytes 524320 | tf_op jit(solution)/shard_map/all_to_all | solution.py:233
  (179 shorter events, 85.3 us)
Async XLA Ops:
  3.4 41.2 %all-to-all-start = ((bf16[64,16,512]{2,1,0:T(8,128)(2,1)}), bf16[64,16,512]{2,1,0:T(8,128)(2,1)S(1)}, u32[]{:S(2)}, u32[]{:S(2)}) async-start(bf16[64,16,512]{2,1,0:T(8,128)(2,1)} %bitcast.70), calls=%async_computation | async-start | bytes 2097152 | tf_op jit(solution)/shard_map/all_to_all | solution.py:233
  45.5 53.0 %all-to-all-start.1 = ((bf16[64,16,512]{2,1,0:T(8,128)(2,1)}), bf16[64,16,512]{2,1,0:T(8,128)(2,1)}, u32[]{:S(2)}, u32[]{:S(2)}) async-start(bf16[64,16,512]{2,1,0:T(8,128)(2,1)} %bitcast.68), calls=%async_computation.1 | async-start | bytes 2097152 | tf_op jit(solution)/shard_map/all_to_all | solution.py:233
  53.4 14.5 %collective-permute-start.1 = (bf16[512,512]{1,0:T(8,128)(2,1)S(1)}, bf16[512,512]{1,0:T(8,128)(2,1)S(1)}, u32[]{:S(2)}, u32[]{:S(2)}) collective-permute-start(bf16[512,512]{1,0:T(8,128)(2,1)S(1)} %get-tuple-element.72.refs_0_.own), channel_id=1, source_target_pairs={{0,1},{1,2},{2,3},{3,0},{4,5},{5,6},{6,7},{7,4},{8,9},{9,10},{10,1... | collective-permute-start | bytes 1572872 | tf_op jit(solution)/shard_map/ppermute | solution.py:227
  54.7 14.4 %collective-permute-start.6 = (bf16[512,512]{1,0:T(8,128)(2,1)S(1)}, bf16[512,512]{1,0:T(8,128)(2,1)S(1)}, u32[]{:S(2)}, u32[]{:S(2)}) collective-permute-start(bf16[512,512]{1,0:T(8,128)(2,1)S(1)} %get-tuple-element.71.refs_8_.own), channel_id=1, source_target_pairs={{0,3},{1,0},{2,1},{3,2},{4,7},{5,4},{6,5},{7,6},{8,11},{9,8},{10,9... | collective-permute-start | bytes 1572872 | tf_op jit(solution)/shard_map/ppermute | solution.py:230
  56.3 22.5 %collective-permute-start = (bf16[512,512]{1,0:T(8,128)(2,1)S(1)}, bf16[512,512]{1,0:T(8,128)(2,1)S(1)}, u32[]{:S(2)}, u32[]{:S(2)}) collective-permute-start(bf16[512,512]{1,0:T(8,128)(2,1)S(1)} %get-tuple-element.72.refs_0_.own), channel_id=1, source_target_pairs={{0,3},{1,0},{2,1},{3,2},{4,7},{5,4},{6,5},{7,6},{8,11},{9,8},{10,9... | collective-permute-start | bytes 1572872 | tf_op jit(solution)/shard_map/ppermute | solution.py:230
  67.8 24.7 %collective-permute-start.8 = (bf16[512,512]{1,0:T(8,128)(2,1)S(1)}, bf16[512,512]{1,0:T(8,128)(2,1)S(1)}, u32[]{:S(2)}, u32[]{:S(2)}) collective-permute-start(bf16[512,512]{1,0:T(8,128)(2,1)S(1)} %get-tuple-element.71.refs_8_.own), channel_id=1, source_target_pairs={{0,1},{1,2},{2,3},{3,0},{4,5},{5,6},{6,7},{7,4},{8,9},{9,10},{10,1... | collective-permute-start | bytes 1572872 | tf_op jit(solution)/shard_map/ppermute | solution.py:227
  69.1 23.5 %collective-permute-start.7 = (bf16[512,512]{1,0:T(8,128)(2,1)S(1)}, bf16[512,512]{1,0:T(8,128)(2,1)S(1)}, u32[]{:S(2)}, u32[]{:S(2)}) collective-permute-start(bf16[512,512]{1,0:T(8,128)(2,1)S(1)} %collective-permute-done.6.refs_9_.right), channel_id=1, source_target_pairs={{0,3},{1,0},{2,1},{3,2},{4,7},{5,4},{6,5},{7,6},{8,11},{9,8},{10,9... | collective-permute-start | bytes 1572872 | tf_op jit(solution)/shard_map/ppermute | solution.py:230
  98.5 83.0 %all-to-all-start.3 = ((bf16[64,8,2048]{2,1,0:T(8,128)(2,1)}), bf16[64,8,2048]{2,1,0:T(8,128)(2,1)}, u32[]{:S(2)}, u32[]{:S(2)}) async-start(bf16[64,8,2048]{2,1,0:T(8,128)(2,1)} %bitcast.69), calls=%async_computation.3 | async-start | bytes 4194304 | tf_op jit(solution)/shard_map/all_to_all | solution.py:233
  112.3 14.3 %collective-permute-start.4 = (bf16[512,512]{1,0:T(8,128)(2,1)S(1)}, bf16[512,512]{1,0:T(8,128)(2,1)S(1)}, u32[]{:S(2)}, u32[]{:S(2)}) collective-permute-start(bf16[512,512]{1,0:T(8,128)(2,1)S(1)} %get-tuple-element.70.refs_4_.own), channel_id=1, source_target_pairs={{0,1},{1,2},{2,3},{3,0},{4,5},{5,6},{6,7},{7,4},{8,9},{9,10},{10,1... | collective-permute-start | bytes 1572872 | tf_op jit(solution)/shard_map/ppermute | solution.py:227
  112.4 14.3 %collective-permute-start.9 = (bf16[512,512]{1,0:T(8,128)(2,1)S(1)}, bf16[512,512]{1,0:T(8,128)(2,1)S(1)}, u32[]{:S(2)}, u32[]{:S(2)}) collective-permute-start(bf16[512,512]{1,0:T(8,128)(2,1)S(1)} %get-tuple-element.69.refs_12_.own), channel_id=1, source_target_pairs={{0,3},{1,0},{2,1},{3,2},{4,7},{5,4},{6,5},{7,6},{8,11},{9,8},{10,9... | collective-permute-start | bytes 1572872 | tf_op jit(solution)/shard_map/ppermute | solution.py:230
  115.0 21.7 %collective-permute-start.3 = (bf16[512,512]{1,0:T(8,128)(2,1)S(1)}, bf16[512,512]{1,0:T(8,128)(2,1)S(1)}, u32[]{:S(2)}, u32[]{:S(2)}) collective-permute-start(bf16[512,512]{1,0:T(8,128)(2,1)S(1)} %get-tuple-element.70.refs_4_.own), channel_id=1, source_target_pairs={{0,3},{1,0},{2,1},{3,2},{4,7},{5,4},{6,5},{7,6},{8,11},{9,8},{10,9... | collective-permute-start | bytes 1572872 | tf_op jit(solution)/shard_map/ppermute | solution.py:230
  126.6 13.5 %collective-permute-start.5 = (bf16[512,512]{1,0:T(8,128)(2,1)S(1)}, bf16[512,512]{1,0:T(8,128)(2,1)S(1)}, u32[]{:S(2)}, u32[]{:S(2)}) collective-permute-start(bf16[512,512]{1,0:T(8,128)(2,1)S(1)} %collective-permute-done.4.refs_7_.left), channel_id=1, source_target_pairs={{0,1},{1,2},{2,3},{3,0},{4,5},{5,6},{6,7},{7,4},{8,9},{9,10},{10,1... | collective-permute-start | bytes 1572872 | tf_op jit(solution)/shard_map/ppermute | solution.py:227
  126.6 24.7 %collective-permute-start.11 = (bf16[512,512]{1,0:T(8,128)(2,1)S(1)}, bf16[512,512]{1,0:T(8,128)(2,1)S(1)}, u32[]{:S(2)}, u32[]{:S(2)}) collective-permute-start(bf16[512,512]{1,0:T(8,128)(2,1)S(1)} %get-tuple-element.69.refs_12_.own), channel_id=1, source_target_pairs={{0,1},{1,2},{2,3},{3,0},{4,5},{5,6},{6,7},{7,4},{8,9},{9,10},{10,1... | collective-permute-start | bytes 1572872 | tf_op jit(solution)/shard_map/ppermute | solution.py:227
  126.6 24.7 %collective-permute-start.10 = (bf16[512,512]{1,0:T(8,128)(2,1)S(1)}, bf16[512,512]{1,0:T(8,128)(2,1)S(1)}, u32[]{:S(2)}, u32[]{:S(2)}) collective-permute-start(bf16[512,512]{1,0:T(8,128)(2,1)S(1)} %collective-permute-done.9.refs_13_.right), channel_id=1, source_target_pairs={{0,3},{1,0},{2,1},{3,2},{4,7},{5,4},{6,5},{7,6},{8,11},{9,8},{10,9... | collective-permute-start | bytes 1572872 | tf_op jit(solution)/shard_map/ppermute | solution.py:230
  155.7 15.9 %collective-permute-start.12 = (bf16[512,512]{1,0:T(8,128)(2,1)}, bf16[512,512]{1,0:T(8,128)(2,1)}, u32[]{:S(2)}, u32[]{:S(2)}) collective-permute-start(bf16[512,512]{1,0:T(8,128)(2,1)} %get-tuple-element.51), channel_id=1, source_target_pairs={{0,1},{1,2},{2,3},{3,0},{4,5},{5,6},{6,7},{7,4},{8,9},{9,10},{10,1... | collective-permute-start | bytes 1572872 | tf_op jit(solution)/shard_map/ppermute | solution.py:227
  171.6 58.5 %collective-permute-start.18 = (bf16[512,128]{1,0:T(8,128)(2,1)}, bf16[512,128]{1,0:T(8,128)(2,1)S(1)}, u32[]{:S(2)}, u32[]{:S(2)}) collective-permute-start(bf16[512,128]{1,0:T(8,128)(2,1)} %get-tuple-element.74), channel_id=1, source_target_pairs={{0,3},{1,0},{2,1},{3,2},{4,7},{5,4},{6,5},{7,6},{8,11},{9,8},{10,9... | collective-permute-start | bytes 393224 | tf_op jit(solution)/shard_map/ppermute | solution.py:230
  181.6 55.2 %all-to-all-start.2 = ((bf16[64,8,512]{2,1,0:T(8,128)(2,1)}), bf16[64,8,512]{2,1,0:T(8,128)(2,1)}, u32[]{:S(2)}, u32[]{:S(2)}) async-start(bf16[64,8,512]{2,1,0:T(8,128)(2,1)} %fusion.6), calls=%async_computation.2 | async-start | bytes 1048576 | tf_op jit(solution)/shard_map/all_to_all | solution.py:233
  202.8 23.9 %collective-permute-start.22 = (bf16[256,128]{1,0:T(8,128)(2,1)S(1)}, bf16[256,128]{1,0:T(8,128)(2,1)S(1)}, u32[]{:S(2)}, u32[]{:S(2)}) collective-permute-start(bf16[256,128]{1,0:T(8,128)(2,1)S(1)} %get-tuple-element.67.m_own), channel_id=1, source_target_pairs={{0,3},{1,0},{2,1},{3,2},{4,7},{5,4},{6,5},{7,6},{8,11},{9,8},{10,9... | collective-permute-start | bytes 196616 | tf_op jit(solution)/shard_map/ppermute | solution.py:230
  205.4 21.5 %collective-permute-start.23 = (bf16[256,128]{1,0:T(8,128)(2,1)S(1)}, bf16[256,128]{1,0:T(8,128)(2,1)S(1)}, u32[]{:S(2)}, u32[]{:S(2)}) collective-permute-start(bf16[256,128]{1,0:T(8,128)(2,1)S(1)} %get-tuple-element.67.m_own), channel_id=1, source_target_pairs={{0,2},{1,3},{2,0},{3,1},{4,6},{5,7},{6,4},{7,5},{8,10},{9,11},{10,... | collective-permute-start | bytes 196616 | tf_op jit(solution)/shard_map/ppermute | solution.py:348
  205.4 23.9 %collective-permute-start.24 = (bf16[256,128]{1,0:T(8,128)(2,1)S(1)}, bf16[256,128]{1,0:T(8,128)(2,1)S(1)}, u32[]{:S(2)}, u32[]{:S(2)}) collective-permute-start(bf16[256,128]{1,0:T(8,128)(2,1)S(1)} %get-tuple-element.67.m_own), channel_id=1, source_target_pairs={{0,1},{1,2},{2,3},{3,0},{4,5},{5,6},{6,7},{7,4},{8,9},{9,10},{10,1... | collective-permute-start | bytes 196616 | tf_op jit(solution)/shard_map/ppermute | solution.py:227
  206.0 29.4 %collective-permute-start.19 = (bf16[512,128]{1,0:T(8,128)(2,1)}, bf16[512,128]{1,0:T(8,128)(2,1)S(1)}, u32[]{:S(2)}, u32[]{:S(2)}) collective-permute-start(bf16[512,128]{1,0:T(8,128)(2,1)} %get-tuple-element.76), channel_id=1, source_target_pairs={{0,2},{1,3},{2,0},{3,1},{4,6},{5,7},{6,4},{7,5},{8,10},{9,11},{10,... | collective-permute-start | bytes 393224 | tf_op jit(solution)/shard_map/ppermute | solution.py:348
  227.0 13.8 %collective-permute-start.15 = (bf16[256,512]{1,0:T(8,128)(2,1)}, bf16[256,512]{1,0:T(8,128)(2,1)S(1)}, u32[]{:S(2)}, u32[]{:S(2)}) collective-permute-start(bf16[256,512]{1,0:T(8,128)(2,1)} %get-tuple-element.56), channel_id=1, source_target_pairs={{0,3},{1,0},{2,1},{3,2},{4,7},{5,4},{6,5},{7,6},{8,11},{9,8},{10,9... | collective-permute-start | bytes 786440 | tf_op jit(solution)/shard_map/ppermute | solution.py:230
  230.1 14.7 %collective-permute-start.17 = (bf16[256,512]{1,0:T(8,128)(2,1)S(1)}, bf16[256,512]{1,0:T(8,128)(2,1)S(1)}, u32[]{:S(2)}, u32[]{:S(2)}) collective-permute-start(bf16[256,512]{1,0:T(8,128)(2,1)S(1)} %get-tuple-element.58), channel_id=1, source_target_pairs={{0,1},{1,2},{2,3},{3,0},{4,5},{5,6},{6,7},{7,4},{8,9},{9,10},{10,1... | collective-permute-start | bytes 786440 | tf_op jit(solution)/shard_map/ppermute | solution.py:227
  264.3 31.6 %all-to-all-start.4 = ((bf16[64,32,128]{2,1,0:T(8,128)(2,1)}), bf16[64,32,128]{2,1,0:T(8,128)(2,1)S(1)}, u32[]{:S(2)}, u32[]{:S(2)}) async-start(bf16[64,32,128]{2,1,0:T(8,128)(2,1)} %bitcast.71), calls=%async_computation.4 | async-start | bytes 1048576 | tf_op jit(solution)/shard_map/all_to_all | solution.py:233
  (64 other events, 1135.4 us)
